TPU v7x, 32 devices: a whole 2x2x4 slice. The times are simulated.
32 devices in a mesh: ep: 16 (over z, x, core), tp: 2 (over y).
Axes of the slice: x: 2, y: 2, z: 4, core: 2. Of those that a mesh axis runs over, the one named last changes fastest.
Arguments:
- tokens: bfloat16 [2048, 2048], P('ep'), may hold values from -6 to 6
- routes: int32 [2048, 2], P('ep'), may hold values from 0 to 3, all different within a row; in each aligned block of 128 rows (0 to 127, 128 to 255, ...) at most 80 rows name the same one
- router_weight: bfloat16 [2048, 4], replicated, may hold values from -0.125 to 0.125
- gate_proj: bfloat16 [16, 2048, 1024], P('ep', None, 'tp'), may hold values from -0.125 to 0.125
- up_proj: bfloat16 [16, 2048, 1024], P('ep', None, 'tp'), may hold values from -0.125 to 0.125
- down_proj: bfloat16 [16, 1024, 2048], P('ep', 'tp'), may hold values from -0.09375 to 0.09375
- cotangent: bfloat16 [2048, 2048], P('ep'), may hold values from -1.5 to 1.5
Outputs:
- token_grad: bfloat16 [2048, 2048], P('ep', 'tp')
- gate_grad: float32 [2048, 2], P('ep')
- router_grad: float32 [2048, 4], P('ep')
- gate_proj_grad: float32 [16, 2048, 1024], P('ep', None, 'tp')
- up_proj_grad: float32 [16, 2048, 1024], P('ep', None, 'tp')
- down_proj_grad: float32 [16, 1024, 2048], P('ep', 'tp')
Inputs may be any that keep to these rules, and one draw needn't show every extreme that they name: `routes`: each row names 2 different experts. Among the rows of one index of ep no expert is named more than 80 times, a bound that some block reaches.
All inputs are finite; a program needn't handle non-finite values.
Results may differ from a plain program's by a relative error of at most 0.0085.
Values may be sent and summed in bfloat16 or wider, within the bound.
No kernel may reach another device: no remote copies, remote signals or barrier semaphores. Data moves between devices by JAX's collectives and lax.ppermute only.
A program may use at most 128 MiB of HBM per device.

v0:
```python
import jax
import jax.numpy as jnp
from jax import lax
from jax.sharding import PartitionSpec as P

MEMBERS = 4
TOP = 2


def shards(tokens, routes, router_weight, gate_proj, up_proj, down_proj, cotangent):
    ntok = tokens.shape[0]
    width = tokens.shape[1]
    experts = router_weight.shape[1]
    n_ep = lax.axis_size("ep")
    n_tp = lax.axis_size("tp")
    share = width // n_tp
    capacity = min(ntok, 5 * TOP * ntok // (4 * experts))
    tp_index = lax.axis_index("tp")
    logits = jnp.dot(tokens, router_weight, preferred_element_type=jnp.float32)
    onehot = (routes[:, :, None] == jnp.arange(experts, dtype=jnp.int32)[None, None, :]).astype(
        jnp.float32
    )
    chosen = jnp.sum(onehot * logits[:, None, :], axis=2)
    first = jax.nn.sigmoid(chosen[:, 0] - chosen[:, 1])
    gates = jnp.stack([first, 1.0 - first], axis=1)
    used = gates.astype(jnp.bfloat16)
    flat = onehot.reshape(ntok * TOP, experts)
    rank = jnp.cumsum(flat, axis=0) - flat
    rank_sel = jnp.sum(flat * rank, axis=1).astype(jnp.int32)
    target = routes.reshape(-1) * capacity + rank_sel
    placing = (jnp.arange(experts * capacity, dtype=jnp.int32)[:, None] == target[None, :]).astype(
        jnp.float32
    )
    place_tok = jnp.sum(placing.reshape(experts * capacity, ntok, TOP), axis=2)
    place_bf = place_tok.astype(jnp.bfloat16)

    def spread(buffer):
        tail = buffer.shape[1:]
        grown = jnp.broadcast_to(
            buffer.reshape((experts, 1, capacity) + tail), (experts, MEMBERS, capacity) + tail
        )
        return grown.reshape((n_ep * capacity,) + tail)

    gate_slots = jnp.dot(
        placing, used.reshape(-1).astype(jnp.float32), precision=lax.Precision.HIGHEST
    ).astype(jnp.bfloat16)
    gate_send = spread(gate_slots[:, None])[:, 0]
    tok_part = lax.dynamic_slice_in_dim(tokens, tp_index * share, share, 1)
    cot_part = lax.dynamic_slice_in_dim(cotangent, tp_index * share, share, 1)
    tok_send = spread(
        jnp.dot(place_bf, tok_part, preferred_element_type=jnp.float32).astype(jnp.bfloat16)
    )
    cot_send = spread(
        jnp.dot(place_bf, cot_part, preferred_element_type=jnp.float32).astype(jnp.bfloat16)
    )
    tok_half, cot_half, gate_rows = (
        lax.all_to_all(tok_send, "ep", split_axis=0, concat_axis=0, tiled=True),
        lax.all_to_all(cot_send, "ep", split_axis=0, concat_axis=0, tiled=True),
        lax.all_to_all(gate_send, "ep", split_axis=0, concat_axis=0, tiled=True),
    )
    tok_rows, cot_rows = (
        lax.all_gather(tok_half, "tp", axis=1, tiled=True),
        lax.all_gather(cot_half, "tp", axis=1, tiled=True),
    )
    w_gate = gate_proj[0]
    w_up = up_proj[0]
    w_down = down_proj[0]
    gpre = jnp.dot(tok_rows, w_gate, preferred_element_type=jnp.float32)
    upre = jnp.dot(tok_rows, w_up, preferred_element_type=jnp.float32)
    sig = jax.nn.sigmoid(gpre)
    silu_val = gpre * sig
    hidden = (silu_val * upre).astype(jnp.bfloat16)
    qvals = lax.dot_general(
        cot_rows, w_down, (((1,), (1,)), ((), ())), preferred_element_type=jnp.float32
    )
    gate_part = jnp.sum(hidden.astype(jnp.float32) * qvals, axis=1)
    weight = gate_rows.astype(jnp.float32)[:, None]
    dhid = weight * qvals
    d_gate = (dhid * upre * sig * (1.0 + gpre * (1.0 - sig))).astype(jnp.bfloat16)
    d_up = (dhid * silu_val).astype(jnp.bfloat16)
    scaled = (weight * hidden.astype(jnp.float32)).astype(jnp.bfloat16)
    grad_down = lax.dot_general(
        scaled, cot_rows, (((0,), (0,)), ((), ())), preferred_element_type=jnp.float32
    )
    grad_gate = lax.dot_general(
        tok_rows, d_gate, (((0,), (0,)), ((), ())), preferred_element_type=jnp.float32
    )
    grad_up = lax.dot_general(
        tok_rows, d_up, (((0,), (0,)), ((), ())), preferred_element_type=jnp.float32
    )
    row_grad = lax.dot_general(
        d_gate, w_gate, (((1,), (1,)), ((), ())), preferred_element_type=jnp.float32
    )
    row_grad = row_grad + lax.dot_general(
        d_up, w_up, (((1,), (1,)), ((), ())), preferred_element_type=jnp.float32
    )
    row_share = lax.psum_scatter(row_grad, "tp", scatter_dimension=1, tiled=True)
    gate_total = lax.psum(gate_part, "tp")
    back_rows, back_gate = (
        lax.all_to_all(row_share, "ep", split_axis=0, concat_axis=0, tiled=True),
        lax.all_to_all(gate_total, "ep", split_axis=0, concat_axis=0, tiled=True),
    )
    back_rows = jnp.sum(back_rows.reshape(experts, MEMBERS, capacity, share), axis=1).reshape(
        experts * capacity, share
    )
    back_gate = jnp.sum(back_gate.reshape(experts, MEMBERS, capacity), axis=1).reshape(
        experts * capacity
    )
    route_sum = lax.dot_general(
        place_tok, back_rows, (((0,), (0,)), ((), ())), precision=lax.Precision.HIGHEST
    )
    gate_grad = lax.dot_general(
        placing, back_gate, (((0,), (0,)), ((), ())), precision=lax.Precision.HIGHEST
    ).reshape(ntok, TOP)
    delta = first * (1.0 - first) * (gate_grad[:, 0] - gate_grad[:, 1])
    dlogits = delta[:, None] * (onehot[:, 0] - onehot[:, 1])
    router_rows = lax.dynamic_slice_in_dim(router_weight, tp_index * share, share, 0).astype(
        jnp.float32
    )
    router_part = lax.dot_general(
        dlogits, router_rows, (((1,), (1,)), ((), ())), precision=lax.Precision.HIGHEST
    )
    token_grad = (route_sum + router_part).astype(jnp.bfloat16)
    columns = tokens.astype(jnp.float32)
    router_grad = lax.psum_scatter(
        lax.dot_general(
            columns, dlogits, (((0,), (0,)), ((), ())), precision=lax.Precision.HIGHEST
        ),
        "ep",
        scatter_dimension=0,
        tiled=True,
    )
    return (token_grad, gate_grad, router_grad, grad_gate[None], grad_up[None], grad_down[None])


def solution(mesh):
    placed = (
        P("ep", None),
        P("ep", None),
        P(),
        P("ep", None, "tp"),
        P("ep", None, "tp"),
        P("ep", "tp", None),
        P("ep", None),
    )
    return jax.shard_map(
        shards,
        mesh=mesh,
        in_specs=placed,
        out_specs=(
            P("ep", "tp"),
            P("ep", None),
            P("ep", None),
            P("ep", None, "tp"),
            P("ep", None, "tp"),
            P("ep", "tp", None),
        ),
        check_vma=False,
    )
```

profile of v0, /device:TPU:11, one launch (start us, length us, event | category | flops | bytes accessed | tf_op | source)
XLA Modules:
  0.0 496.3 jit_solution(1121042243303813282)
XLA Ops:
  7.2 0.0 copy-start
  7.2 0.0 all-gather.5.cloned.1.call-start
  7.2 0.9 copy.58
  8.2 0.1 eq.68
  8.3 0.1 eq.72
  8.5 1.2 reduce-window.6
  9.7 0.1 slice.32
  9.8 0.1 copy.60
  9.9 0.1 copy.61
  10.0 0.1 add_bitcast_fusion
  10.1 0.1 convert_element_type.77
  10.3 0.1 copy.62
  10.3 0.7 multiply_add_fusion.1
  11.1 0.0 copy-start.4
  11.1 1.3 convolution_convert_fusion
  12.4 0.3 broadcast_in_dim.42
  12.8 64.9 %all_to_all.51 = bf16[16,80,1024]{2,1,0:T(8,128)(2,1)} all-to-all(bf16[16,80,1024]{2,1,0:T(8,128)(2,1)S(1)} %bitcast.86), channel_id=1, replica_groups=mesh['ep'=16,'tp'=2] {'ep'}, dimensions={0} | all-to-all | bytes 5242880 | tf_op jit(solution)/shard_map/all_to_all | solution.py:57
  77.7 0.0 all-gather.5.cloned.1.call-update
  77.7 0.0 all-gather.3.cloned.1.call-start
  77.8 1.0 copy-done.8
  78.7 0.3 convolution_convert_fusion.1
  79.1 0.3 broadcast_in_dim.40
  79.4 63.8 %all_to_all.52 = bf16[16,80,1024]{2,1,0:T(8,128)(2,1)} all-to-all(bf16[16,80,1024]{2,1,0:T(8,128)(2,1)S(1)} %bitcast.87), channel_id=1, replica_groups=mesh['ep'=16,'tp'=2] {'ep'}, dimensions={0} | all-to-all | bytes 5242880 | tf_op jit(solution)/shard_map/all_to_all | solution.py:58
  143.2 0.0 all-gather.3.cloned.1.call-update
  143.2 0.0 reduce-scatter.5.cloned.1.call-start
  143.2 1.0 copy-done.2
  144.2 0.2 fusion.37
  144.5 0.1 copy.63
  144.7 0.2 reshape.132
  144.8 0.2 convolution_reduce_fusion
  145.0 0.1 broadcast_in_dim.18
  145.1 8.4 %all_to_all.53 = bf16[16,80,1]{1,2,0:T(2,128)(2,1)S(1)} all-to-all(bf16[16,80,1]{1,2,0:T(2,128)(2,1)S(1)} %copy.64), channel_id=1, replica_groups=mesh['ep'=16,'tp'=2] {'ep'}, dimensions={0} | all-to-all | bytes 5120 | tf_op jit(solution)/shard_map/all_to_all | solution.py:59
  153.6 0.1 reshape.131
  153.7 0.0 copy-start.6
  153.7 7.8 %fusion.5 = f32[1280,512]{0,1:T(8,128)} fusion(bf16[1280,2048]{1,0:T(8,128)(2,1)} %all-gather.5.cloned.1.call-done, bf16[1,2048,512]{2,1,0:T(8,128)(2,1)S(1)} %copy-done), kind=kOutput, calls=%fused_computation.17 | convolution fusion | flops 2684354560 | bytes 9961472 | tf_op jit(solution)/shard_map/dot_general | solution.py:68
  161.5 4.6 fusion.8
  166.1 49.9 %all-gather.3.cloned.1.call-done = bf16[1280,2048]{1,0:T(8,128)(2,1)} async-done(((bf16[1280,1024]{1,0:T(8,128)(2,1)}), bf16[1280,2048]{1,0:T(8,128)(2,1)}) %all-gather.3.cloned.1.call-update) | async-done | bytes 5242896 | tf_op jit(solution)/shard_map/all_gather | solution.py:63
  216.1 9.6 %fusion = (f32[1280]{0:T(1024)S(1)}, bf16[1280,512]{0,1:T(8,128)(2,1)}, bf16[1280,512]{0,1:T(8,128)(2,1)S(1)}, bf16[1280,512]{0,1:T(8,128)(2,1)S(1)}) fusion(f32[1280,512]{0,1:T(8,128)} %fusion.8, f32[1280,512]{0,1:T(8,128)} %fusion.5, f32[1280]{0:T(1024)S(1)} %reshape.131, bf16[1280,2048]{1,0:T(8,128)(2,1)} %all-gather.3.cloned.1.call-done, ...), kind=kOutput, calls=%fused_computation.7 | convolution fusion | flops 2696805120 | bytes 16525312 | tf_op jit(solution)/shard_map/dot_general | solution.py:73
  225.7 3.2 fusion.3
  228.9 5.6 %convolution_add_fusion = f32[1280,2048]{1,0:T(8,128)} fusion(f32[1280,2048]{1,0:T(8,128)S(1)} %fusion.3, bf16[1280,512]{0,1:T(8,128)(2,1)S(1)} %get-tuple-element.11, bf16[1,2048,512]{2,1,0:T(8,128)(2,1)S(1)} %copy-done.7), kind=kOutput, calls=%fused_computation | convolution fusion | flops 2686976000 | bytes 24379392 | tf_op jit(solution)/shard_map/dot_general | solution.py:94
  234.5 0.0 reduce-scatter.5.cloned.1.call-update
  234.5 0.1 all_to_all.44
  234.6 3.8 psum.7
  238.4 11.4 %all_to_all.54 = f32[16,80,1]{1,2,0:T(1,128)S(1)} all-to-all(f32[16,80,1]{1,2,0:T(1,128)S(1)} %bitcast.93), channel_id=1, replica_groups=mesh['ep'=16,'tp'=2] {'ep'}, dimensions={0} | all-to-all | bytes 10240 | tf_op jit(solution)/shard_map/all_to_all | solution.py:101
  249.8 106.8 %reduce-scatter.5.cloned.1.call-done = f32[1280,1024]{1,0:T(8,128)} async-done(((f32[1280,2048]{1,0:T(8,128)}), f32[1280,1024]{1,0:T(8,128)}) %reduce-scatter.5.cloned.1.call-update) | async-done | bytes 5242896 | tf_op jit(solution)/shard_map/reduce_scatter | solution.py:97
  356.6 6.6 %all-to-all-start.3 = ((f32[16,80,1024]{2,1,0:T(8,128)}), f32[16,80,1024]{2,1,0:T(8,128)}, u32[]{:S(2)}, u32[]{:S(2)}) async-start(f32[16,80,1024]{2,1,0:T(8,128)} %bitcast.88), calls=%async_computation.4 | async-start | bytes 10485760 | tf_op jit(solution)/shard_map/all_to_all | solution.py:100
  363.3 0.0 reduce-scatter.7.cloned.1.call-start
  363.3 0.1 iota_compare_fusion
  363.4 0.1 eq.87
  363.6 7.2 %convolution_bitcast_fusion.2 = f32[1,2048,512]{2,1,0:T(8,128)} fusion(bf16[1280,2048]{1,0:T(8,128)(2,1)} %all-gather.5.cloned.1.call-done, bf16[1280,512]{0,1:T(8,128)(2,1)S(1)} %copy-done.14), kind=kOutput, calls=%fused_computation.6 | convolution fusion | flops 2684354560 | bytes 10747904 | tf_op jit(solution)/shard_map/dot_general | solution.py:85
  370.9 7.2 %convolution_bitcast_fusion.1 = f32[1,2048,512]{2,1,0:T(8,128)} fusion(bf16[1280,2048]{1,0:T(8,128)(2,1)} %all-gather.5.cloned.1.call-done, bf16[1280,512]{0,1:T(8,128)(2,1)S(1)} %get-tuple-element.11), kind=kOutput, calls=%fused_computation.5 | convolution fusion | flops 2684354560 | bytes 10747904 | tf_op jit(solution)/shard_map/dot_general | solution.py:88
  378.1 4.5 convolution_bitcast_fusion
  382.6 0.1 reshape.130
  382.7 0.4 fusion.15
  383.0 0.1 copy.70
  383.1 0.3 convolution_bitcast_fusion.3
  383.4 1.4 copy.71
  384.8 0.0 reduce-scatter.7.cloned.1.call-update
  384.9 0.4 fusion.21
  385.3 85.3 %reduce-scatter.7.cloned.1.call-done = f32[128,4]{1,0:T(8,128)} async-done(((f32[2048,4]{1,0:T(8,128)}), f32[128,4]{1,0:T(8,128)}) %reduce-scatter.7.cloned.1.call-update) | async-done | bytes 2064
  470.7 1.5 copy.72
  472.2 12.4 %all-to-all-done.3 = f32[16,80,1024]{2,1,0:T(8,128)} async-done(((f32[16,80,1024]{2,1,0:T(8,128)}), f32[16,80,1024]{2,1,0:T(8,128)}, u32[]{:S(2)}, u32[]{:S(2)}) %all-to-all-start.3) | async-done | bytes 5242912 | tf_op jit(solution)/shard_map/all_to_all | solution.py:100
  484.6 3.3 bitcast_reduce_fusion
  487.9 1.8 fusion.14
  (50 shorter events, 0.3 us)
Async XLA Ops:
  7.2 146.5 %copy-start = (bf16[1,2048,512]{2,1,0:T(8,128)(2,1)S(1)}, bf16[1,2048,512]{2,1,0:T(8,128)(2,1)}, u32[]{:S(2)}) copy-start(bf16[1,2048,512]{2,1,0:T(8,128)(2,1)} %param.10) | copy-start | bytes 6291460
  7.2 146.5 %all-gather.5.cloned.1.call-start = ((), (), s32[]{:S(2)}) async-start(), calls=%async_computation.8 | async-start | bytes 7864320 | tf_op jit(solution)/shard_map/all_gather | solution.py:62
  11.1 66.7 %copy-start.4 = (f32[320,128]{1,0:T(8,128)}, f32[320,128]{1,0:T(8,128)S(1)}, u32[]{:S(2)}) copy-start(f32[320,128]{1,0:T(8,128)S(1)} %convert_reduce_fusion) | copy-start | bytes 491524
  77.7 1.0 copy-start.8
  77.7 138.4 %all-gather.3.cloned.1.call-start = ((), (), s32[]{:S(2)}) async-start(), calls=%async_computation.7 | async-start | bytes 7864320 | tf_op jit(solution)/shard_map/all_gather | solution.py:63
  143.2 1.0 copy-start.2
  143.2 1.0 copy-start.9
  143.2 1.3 copy-start.10
  143.2 213.4 %reduce-scatter.5.cloned.1.call-start = ((), (), s32[]{:S(2)}) async-start(), calls=%async_computation.9 | async-start | bytes 15728640 | tf_op jit(solution)/shard_map/reduce_scatter | solution.py:97
  153.7 7.8 %copy-start.6 = (bf16[1,2048,512]{2,1,0:T(8,128)(2,1)S(1)}, bf16[1,2048,512]{2,1,0:T(8,128)(2,1)}, u32[]{:S(2)}) copy-start(bf16[1,2048,512]{2,1,0:T(8,128)(2,1)} %param.11) | copy-start | bytes 6291460
  153.7 7.8 %copy-start.12 = (bf16[1280,2048]{1,0:T(8,128)(2,1)S(1)}, bf16[1280,2048]{1,0:T(8,128)(2,1)}, u32[]{:S(2)}) copy-start(bf16[1280,2048]{1,0:T(8,128)(2,1)} %all-gather.5.cloned.1.call-done) | copy-start | bytes 15728644
  225.7 3.2 copy-start.13
  225.7 3.2 copy-start.7
  356.6 7.0 %copy-start.14 = (bf16[1280,512]{0,1:T(8,128)(2,1)S(1)}, bf16[1280,512]{0,1:T(8,128)(2,1)}, u32[]{:S(2)}) copy-start(bf16[1280,512]{0,1:T(8,128)(2,1)} %copy-done.13) | copy-start | bytes 3932164
  356.6 127.9 %all-to-all-start.3 = ((f32[16,80,1024]{2,1,0:T(8,128)}), f32[16,80,1024]{2,1,0:T(8,128)}, u32[]{:S(2)}, u32[]{:S(2)}) async-start(f32[16,80,1024]{2,1,0:T(8,128)} %bitcast.88), calls=%async_computation.4 | async-start | bytes 10485760 | tf_op jit(solution)/shard_map/all_to_all | solution.py:100
  363.3 107.4 %reduce-scatter.7.cloned.1.call-start = ((), (), s32[]{:S(2)}) async-start(), calls=%async_computation.10 | async-start | bytes 1114112
  363.6 14.5 %slice-start = ((s8[5242880]{0:T(1024)(128)(4,1)}), s8[4194304]{0:T(1024)(128)(4,1)S(1)}, s32[]{:S(2)}) async-start(s8[5242880]{0:T(1024)(128)(4,1)} %bitcast.96), calls=%async_computation.11 | async-start | bytes 8388608
  370.9 7.2 %slice-start.1 = ((s8[5242880]{0:T(1024)(128)(4,1)}), s8[1048576]{0:T(1024)(128)(4,1)S(1)}, s32[]{:S(2)}) async-start(s8[5242880]{0:T(1024)(128)(4,1)} %bitcast.96), calls=%async_computation.12 | async-start | bytes 2097152
  370.9 7.2 %copy-start.15 = (bf16[1280,512]{0,1:T(8,128)(2,1)S(1)}, bf16[1280,512]{0,1:T(8,128)(2,1)}, u32[]{:S(2)}) copy-start(bf16[1280,512]{0,1:T(8,128)(2,1)} %get-tuple-element.9) | copy-start | bytes 3932164
  378.1 5.0 %copy-start.3 = (bf16[128,2048]{1,0:T(8,128)(2,1)S(1)}, bf16[128,2048]{1,0:T(8,128)(2,1)}, u32[]{:S(2)}) copy-start(bf16[128,2048]{1,0:T(8,128)(2,1)} %param.7) | copy-start | bytes 1572868
  383.1 104.8 %copy-start.11 = (f32[128,2]{0,1:T(2,128)}, f32[128,2]{0,1:T(2,128)S(1)}, u32[]{:S(2)}) copy-start(f32[128,2]{0,1:T(2,128)S(1)} %copy.70) | copy-start | bytes 3076
  472.2 15.8 %copy-start.5 = (f32[320,128]{1,0:T(8,128)S(1)}, f32[320,128]{1,0:T(8,128)}, u32[]{:S(2)}) copy-start(f32[320,128]{1,0:T(8,128)} %copy-done.4) | copy-start | bytes 491524
  484.6 5.2 %copy-start.1 = (bf16[1,2048,512]{2,1,0:T(8,128)(2,1)S(1)}, bf16[1,2048,512]{2,1,0:T(8,128)(2,1)}, u32[]{:S(2)}) copy-start(bf16[1,2048,512]{2,1,0:T(8,128)(2,1)} %param.10) | copy-start | bytes 6291460
Sparse Core Ops, SparseCore 0:
  77.8 68.0 all-gather.4
  147.5 68.5 all-gather.2
  234.7 121.9 reduce-scatter.4
  385.0 85.6 reduce-scatter.6
where the time goes:
time: 497 us; the launch traced here: 496 us
  waiting for transfers between devices  255 us (51%)
  blocking collectives  152 us (31%)
  matrix products  54.4 us (11%)
  between operations  14.1 us (3%)
  local copies, waits for them, and re-layouts  8.03 us (2%)
  starting transfers between devices  6.8 us (1%)
  other arithmetic  6.04 us (1%)
    reduce_scatter x1, waiting for transfers between devices, shards(): lax.psum_scatter(row_grad, 'tp', scatter_dimension=1, tiled=True)  107 us
    unnamed x5, waiting for transfers between devices  85.4 us
    all_to_all x1, blocking collectives, shards(): lax.all_to_all(tok_send, 'ep', split_axis=0, concat_axis=0, tiled=True)  64.9 us
    all_to_all x1, blocking collectives, shards(): lax.all_to_all(cot_send, 'ep', split_axis=0, concat_axis=0, tiled=True)  63.8 us
    all_gather x1, waiting for transfers between devices, shards(): lax.all_gather(cot_half, 'tp', axis=1, tiled=True)  49.9 us
    all_to_all x1, waiting for transfers between devices, shards(): lax.all_to_all(row_share, 'ep', split_axis=0, concat_axis=0, tiled=True)  12.4 us
    all_to_all x1, blocking collectives, shards(): lax.all_to_all(gate_total, 'ep', split_axis=0, concat_axis=0, tiled=True)  11.4 us
  transfers between devices with their start and end apart: 5, of which 4 were waited for; matrix products, arithmetic and copies ran while one was open for 8% of the time, Pallas kernels for 0%

commit v1 on v0

v1 whole, which is shorter than its diff:
```python
import functools

import jax
import jax.numpy as jnp
from jax import lax
from jax.experimental import pallas as pl
from jax.experimental.pallas import tpu as pltpu
from jax.sharding import PartitionSpec as P


MEMBERS = 4
TOP = 2
LANES = 128
TILE = 16
MIB = 1024 * 1024


f32, bf16, i32 = jnp.float32, jnp.bfloat16, jnp.int32
ACROSS = (((0,), (0,)), ((), ()))
BACK = (((1,), (1,)), ((), ()))
WHOLE = pl.BlockSpec(memory_space=pltpu.VMEM)
SCALARS = pl.BlockSpec(memory_space=pltpu.SMEM)


def mxu(a, b, dims=(((1,), (0,)), ((), ())), precision=None):
    return lax.dot_general(a, b, dims, preferred_element_type=f32, precision=precision)


def call(body, outs, args, limit=60, flops=0, moved=0, **kwargs):
    return pl.pallas_call(
        body,
        out_shape=outs,
        compiler_params=pltpu.CompilerParams(vmem_limit_bytes=limit * MIB),
        cost_estimate=pl.CostEstimate(
            flops=int(flops), bytes_accessed=int(moved), transcendentals=0
        ),
        **kwargs,
    )(*args)


def place_kernel(experts, cap, share, at_ref, routes_ref, tok_ref, cot_ref, place_ref, *outs):
    mine, start = at_ref[0], pl.multiple_of(at_ref[1] * share, LANES)
    ntok = routes_ref.shape[1]
    tall = -(-experts // TILE) * TILE
    kind = lax.broadcasted_iota(i32, (tall, ntok), 0)
    named = jnp.zeros((tall, ntok), f32)
    for k in range(TOP):
        away = routes_ref[k : k + 1, :] - mine
        away = jnp.where(away < 0, away + experts, away)
        named = named + jnp.where(kind == away, 1.0, 0.0)
    row = lax.broadcasted_iota(i32, (ntok, ntok), 0)
    column = lax.broadcasted_iota(i32, (ntok, ntok), 1)
    rank = mxu(named.astype(bf16), jnp.where(row < column, 1.0, 0.0).astype(bf16))
    rank = jnp.where(named > 0.5, rank, -1.0)
    slot = lax.broadcasted_iota(i32, (cap, ntok), 0).astype(f32)
    tok = tok_ref[:, pl.ds(start, share)]
    cot = cot_ref[:, pl.ds(start, share)]
    for d in range(experts):
        place = jnp.where(slot == rank[d : d + 1], 1.0, 0.0).astype(bf16)
        place_ref[d] = place
        outs[d][...] = mxu(place, tok).astype(bf16)
        outs[experts + d][...] = mxu(place, cot).astype(bf16)


def terms(value):
    parts = []
    for _ in range(3):
        parts.append(value.astype(bf16))
        value = value - parts[-1].astype(f32)
    return parts


def gates_kernel(experts, cap, at_ref, routes_ref, tok_ref, router_ref, place_ref, first_ref, *outs):
    logits = mxu(router_ref[...], tok_ref[...], BACK)
    ntok, lanes = logits.shape[1], outs[0].shape[1]
    kind = lax.broadcasted_iota(i32, (experts, ntok), 0)
    chosen = [
        jnp.sum(jnp.where(kind == routes_ref[k : k + 1, :], logits, 0.0), axis=0, keepdims=True)
        for k in range(TOP)
    ]
    first = jax.nn.sigmoid(chosen[0] - chosen[1])
    first_ref[...] = first
    used = [first.astype(bf16).astype(f32), (1.0 - first).astype(bf16).astype(f32)]
    for d in range(experts):
        value = jnp.zeros((1, ntok), f32)
        for k in range(TOP):
            away = routes_ref[k : k + 1, :] - at_ref[0]
            away = jnp.where(away < 0, away + experts, away)
            value = value + jnp.where(away == d, used[k], 0.0)
        value = jnp.broadcast_to(value, (8, ntok)).astype(bf16)
        slots = mxu(value, place_ref[d], BACK)[:1]
        outs[d][...] = jnp.zeros((1, lanes), f32)
        outs[d][:, :cap] = slots


def expert_kernel(
    layout, n_tp, share, tp_ref, tok_ref, cot_ref, gate_ref, wg_ref, wu_ref, wd_ref,
    dg_ref, du_ref, sc_ref, rg_ref, part_ref,
):
    group, experts, cap = layout
    rows, lanes = tok_ref.shape[0], gate_ref.shape[1]
    step = pl.program_id(0)
    starts = [
        pl.multiple_of(lax.rem(tp_ref[0] - k + n_tp, n_tp) * share, LANES) for k in range(n_tp)
    ]
    spans = [slice(k * share, (k + 1) * share) for k in range(n_tp)]
    gpre = sum(mxu(tok_ref[:, s], wg_ref[pl.ds(a, share), :]) for s, a in zip(spans, starts))
    upre = sum(mxu(tok_ref[:, s], wu_ref[pl.ds(a, share), :]) for s, a in zip(spans, starts))
    qvals = sum(
        mxu(cot_ref[:, s], wd_ref[:, pl.ds(a, share)], BACK) for s, a in zip(spans, starts)
    )

    entry = lax.broadcasted_iota(i32, (1, 2 * experts), 1)
    low = jnp.full((1, 2 * experts), -cap, i32)
    for i in range(2):
        for at, d in enumerate(group):
            low = jnp.where(entry == i * experts + d, (i * len(group) + at) * cap, low)
    row = lax.broadcasted_iota(i32, (rows, 1), 0) + step * rows
    mine = (row >= low) & (row < low + cap)
    slot = row - jnp.sum(jnp.where(mine, low, 0), axis=1, keepdims=True)
    mine = jnp.where(mine, 1.0, 0.0)
    seat = lax.broadcasted_iota(i32, (rows, lanes), 1) == slot
    weight = mxu(mine.astype(bf16), gate_ref[...].astype(bf16))
    weight = jnp.sum(jnp.where(seat, weight, 0.0), axis=1, keepdims=True)

    sig = jax.nn.sigmoid(gpre)
    silu_val = gpre * sig
    hidden = (silu_val * upre).astype(bf16)
    wide = hidden.astype(f32)
    part = jnp.sum(wide * qvals, axis=1, keepdims=True)
    ones = mine.astype(bf16)
    part = sum(mxu(ones, term, ACROSS) for term in terms(jnp.where(seat, part, 0.0)))

    @pl.when(step == 0)
    def _():
        part_ref[...] = part

    @pl.when(step > 0)
    def _():
        part_ref[...] += part

    dhid = weight * qvals
    d_gate = (dhid * upre * sig * (1.0 + gpre * (1.0 - sig))).astype(bf16)
    d_up = (dhid * silu_val).astype(bf16)
    dg_ref[...] = d_gate
    du_ref[...] = d_up
    sc_ref[...] = (weight * wide).astype(bf16)
    for s, a in zip(spans, starts):
        total = mxu(d_gate, wg_ref[pl.ds(a, share), :], BACK)
        total = total + mxu(d_up, wu_ref[pl.ds(a, share), :], BACK)
        rg_ref[:, s] = total.astype(bf16)


def parts_kernel(experts, n, at_ref, *refs):
    out = refs[2 * n]
    mine, member = at_ref[0], at_ref[2]
    n_ep, lanes = out.shape[0], out.shape[2]
    entry = lax.broadcasted_iota(i32, (1, 2 * experts), 1)
    i = jnp.where(entry >= experts, 1, 0)
    away = mine - (entry - i * experts)
    away = jnp.where(away < 0, away + experts, away)
    device = lax.broadcasted_iota(i32, (n_ep, 2 * experts), 0)
    total = jnp.zeros((n_ep, lanes), f32)
    for j in range(2):
        table = refs[j * n][...]
        for c in range(1, n):
            table = table + refs[j * n + c][...]
        owner = away * MEMBERS + jnp.bitwise_xor(member, 2 * i + j)
        pick = jnp.where(device == owner, 1.0, 0.0).astype(bf16)
        total = total + sum(mxu(pick, term) for term in terms(table))
    for e in range(n_ep):
        out[e] = total[e : e + 1, :]


def router_kernel(
    experts, cap, n, at_ref, routes_ref, tok_ref, place_ref, first_ref, *refs
):
    gate_ref, change_ref, out_ref = refs[n:]
    ntok = routes_ref.shape[1]
    values = []
    for d in range(experts):
        source = lax.rem(at_ref[0] + d, experts)
        back = refs[0][pl.ds(source, 1), :]
        for ref in refs[1:n]:
            back = back + ref[pl.ds(source, 1), :]
        back = jnp.broadcast_to(back[:, :cap], (8, cap))
        values.append(sum(mxu(term, place_ref[d]) for term in terms(back))[:1])
    grads = []
    for k in range(TOP):
        away = routes_ref[k : k + 1, :] - at_ref[0]
        away = jnp.where(away < 0, away + experts, away)
        value = jnp.zeros((1, ntok), f32)
        for d in range(experts):
            value = value + jnp.where(away == d, values[d], 0.0)
        gate_ref[k : k + 1, :] = value
        grads.append(value)
    first = first_ref[...]
    delta = first * (1.0 - first) * (grads[0] - grads[1])
    kind = lax.broadcasted_iota(i32, (experts, ntok), 0)
    change = jnp.where(kind == routes_ref[0:1, :], delta, 0.0)
    change = change - jnp.where(kind == routes_ref[1:2, :], delta, 0.0)
    change_ref[...] = change
    total = sum(mxu(term, tok_ref[...]) for term in terms(change))
    n_ep, span = out_ref.shape[0], out_ref.shape[2]
    for e in range(n_ep):
        out_ref[e] = total[:, e * span : (e + 1) * span]


def pair_kernel(counts, n_tp, share, *refs):
    n = len(counts)
    outs = refs[2 * n :]
    low = 0
    for c, rows in enumerate(counts):
        for i in range(2):
            for k in range(n_tp):
                piece = (slice(i * rows, (i + 1) * rows), slice(k * share, (k + 1) * share))
                total = refs[2 * c][piece].astype(f32) + refs[2 * c + 1][piece].astype(f32)
                outs[i * n_tp + k][low : low + rows, :] = total.astype(bf16)
        low += rows


def total_kernel(n, cap, *refs):
    outs = refs[n:]
    for at, out in enumerate(outs):
        piece = slice(at * cap, (at + 1) * cap)
        total = refs[0][piece, :].astype(f32)
        for ref in refs[1:n]:
            total = total + ref[piece, :].astype(f32)
        out[...] = total.astype(bf16)


def token_kernel(experts, share, at_ref, place_ref, change_ref, router_ref, *refs):
    start = pl.multiple_of(at_ref[1] * share, LANES)
    router = router_ref[:, pl.ds(start, share)]
    total = sum(mxu(term, router, ACROSS) for term in terms(change_ref[...]))
    for d in range(experts):
        total = total + mxu(place_ref[d], refs[d][...], ACROSS)
    refs[experts][...] = total.astype(bf16)


def in_grads_kernel(n, tp_ref, *refs):
    gate_ref, up_ref, tok_all, gates, ups = refs[3 * n :]

    def gather(refs, target):
        low = 0
        for ref in refs:
            target[low : low + ref.shape[0], :] = ref[...]
            low += ref.shape[0]

    @pl.when(pl.program_id(0) == 0)
    def _():
        gather(refs[n : 2 * n], gates)
        gather(refs[2 * n : 3 * n], ups)

    gather(refs[:n], tok_all)
    flipped = tok_all[...].T
    gate_ref[...] = mxu(flipped, gates[...])
    up_ref[...] = mxu(flipped, ups[...])


def out_grad_kernel(n, tp_ref, *refs):
    down_ref, cot_all, scaled = refs[2 * n :]
    low = 0
    for ref in refs[:n]:
        cot_all[low : low + ref.shape[0], :] = ref[...]
        low += ref.shape[0]

    @pl.when(pl.program_id(0) == 0)
    def _():
        low = 0
        for ref in refs[n : 2 * n]:
            scaled[:, low : low + ref.shape[0]] = ref[...].T
            low += ref.shape[0]

    down_ref[...] = mxu(scaled[...], cot_all[...])


def grouped(experts):
    near = sorted({0, 1 % experts, (experts - 1) % experts})
    rest = [d for d in range(experts) if d not in near]
    return [near] + ([rest] if rest else [])


def shards(tokens, routes, router_weight, gate_proj, up_proj, down_proj, cotangent):
    ntok, width = tokens.shape
    experts = router_weight.shape[1]
    n_ep = lax.axis_size("ep")
    n_tp = lax.axis_size("tp")
    share = width // n_tp
    hidden_units = gate_proj.shape[2]
    cap = min(ntok, 5 * TOP * ntok // (4 * experts))
    cap = -(-cap // TILE) * TILE
    lanes = -(-cap // LANES) * LANES
    tp = lax.axis_index("tp")
    ep = lax.axis_index("ep")
    mine = ep // MEMBERS
    member = ep % MEMBERS
    groups = grouped(experts)
    shape = jax.ShapeDtypeStruct

    def flip(value, bit):
        return lax.ppermute(value, "ep", [(i, i ^ bit) for i in range(n_ep)])

    def shift(value, step):
        pairs = [(i, (i + step * MEMBERS) % n_ep) for i in range(n_ep)]
        return lax.ppermute(value, "ep", pairs)

    def turn(value, step):
        return lax.ppermute(value, "tp", [(i, (i + step) % n_tp) for i in range(n_tp)])

    def direct(value, bit, step):
        pairs = [
            (i * n_tp + j, (i ^ bit) * n_tp + (j + step) % n_tp)
            for i in range(n_ep)
            for j in range(n_tp)
        ]
        return lax.ppermute(value, ("ep", "tp"), pairs)

    def spread(value):
        return [value] + [turn(value, k) for k in range(1, n_tp)]

    at = jnp.stack([mine, tp, member]).astype(i32)
    router = router_weight.T

    placed = call(
        functools.partial(place_kernel, experts, cap, share),
        [shape((experts, cap, ntok), bf16)] + [shape((cap, share), bf16)] * (2 * experts),
        (at, routes.T, tokens, cotangent),
        in_specs=[SCALARS] + [WHOLE] * 3,
        out_specs=[WHOLE] * (1 + 2 * experts),
        flops=4 * experts * cap * ntok * share,
        moved=4 * ntok * width,
    )
    place, tok_send, cot_send = placed[0], placed[1 : 1 + experts], placed[1 + experts :]
    arrived = {0: (tok_send[0], cot_send[0])}
    for d in range(1, experts):
        arrived[d] = (shift(tok_send[d], d), shift(cot_send[d], d))

    first, *gate_slots = call(
        functools.partial(gates_kernel, experts, cap),
        [shape((1, ntok), f32)] + [shape((1, lanes), f32)] * experts,
        (at, routes.T, tokens, router, place),
        in_specs=[SCALARS] + [WHOLE] * 4,
        out_specs=[WHOLE] * (1 + experts),
        flops=4 * ntok * width * LANES,
        moved=2 * ntok * width,
    )
    gate_rows = jnp.concatenate(
        gate_slots[:1] + [shift(gate_slots[d], d) for d in range(1, experts)], axis=0
    )
    gate_chip = jnp.concatenate([gate_rows, flip(gate_rows, 2)], axis=0)
    gate_tables = (gate_chip, flip(gate_chip, 1))

    sent = []
    for group in groups:
        tok, cot = arrived[group[0]]
        if len(group) > 1:
            tok = jnp.concatenate([arrived[d][0] for d in group], axis=0)
            cot = jnp.concatenate([arrived[d][1] for d in group], axis=0)
        tok_near, cot_near = spread(tok), spread(cot)
        tok_far = spread(flip(tok, 2))
        cot_far = [flip(piece, 2) for piece in cot_near]
        tok_chip = jnp.concatenate(
            [jnp.concatenate(tok_near, axis=1), jnp.concatenate(tok_far, axis=1)], axis=0
        )
        cot_chip = jnp.concatenate(
            [jnp.concatenate(cot_near, axis=1), jnp.concatenate(cot_far, axis=1)], axis=0
        )
        sent.append(((tok_chip, cot_chip), (flip(tok_chip, 1), flip(cot_chip, 1))))

    w_gate, w_up, w_down = gate_proj[0], up_proj[0], down_proj[0]
    at_tp = tp.astype(i32).reshape(1)

    def experts_on(group, rows_of, gate_table):
        tok, cot = rows_of
        rows = tok.shape[0]
        block = rows if rows <= 512 else rows // 2
        across = lambda s, tp_ref: (s, 0)
        still = lambda s, tp_ref: (0, 0)
        wide = pl.BlockSpec((block, width), across)
        narrow = pl.BlockSpec((block, hidden_units), across)
        return call(
            functools.partial(expert_kernel, (group, experts, cap), n_tp, share),
            [shape((rows, hidden_units), bf16)] * 3
            + [shape((rows, width), bf16), shape((2 * experts, lanes), f32)],
            (at_tp, tok, cot, gate_table, w_gate, w_up, w_down),
            limit=36,
            flops=10 * rows * width * hidden_units,
            moved=6 * rows * width + 6 * width * hidden_units,
            grid_spec=pltpu.PrefetchScalarGridSpec(
                num_scalar_prefetch=1,
                grid=(rows // block,),
                in_specs=[wide, wide, pl.BlockSpec((2 * experts, lanes), still)]
                + [pl.BlockSpec((width, hidden_units), still)] * 2
                + [pl.BlockSpec((hidden_units, width), still)],
                out_specs=[narrow] * 3 + [wide, pl.BlockSpec((2 * experts, lanes), still)],
            ),
        )

    toks, cots, dgs, dus, scs, parts, grads = [], [], [], [], [], ([], []), []
    for group, pair in zip(groups, sent):
        here = []
        for j in range(2):
            dg, du, sc, rg, part = experts_on(group, pair[j], gate_tables[j])
            toks.append(pair[j][0])
            cots.append(pair[j][1])
            dgs.append(dg)
            dus.append(du)
            scs.append(sc)
            parts[j].append(part)
            here.append(rg)
        grads.append((here[0], flip(here[1], 1)))

    backs = {}
    last = len(groups) - 1
    for chunk in [[c] for c in range(last + 1)]:
        members = [d for c in chunk for d in groups[c]]
        counts = [len(groups[c]) * cap for c in chunk]
        rows = sum(counts)
        pieces = call(
            functools.partial(pair_kernel, counts, n_tp, share),
            [shape((rows, share), bf16)] * (2 * n_tp),
            [value for c in chunk for value in grads[c]],
            in_specs=[WHOLE] * (2 * len(chunk)),
            out_specs=[WHOLE] * (2 * n_tp),
            flops=2 * rows * width,
            moved=12 * rows * width,
        )
        pieces = [
            direct(pieces[i * n_tp + k], 2 * i, -k) if i or k else pieces[0]
            for i in range(2)
            for k in range(n_tp)
        ]
        totals = call(
            functools.partial(total_kernel, 2 * n_tp, cap),
            [shape((cap, share), bf16)] * len(members),
            pieces,
            in_specs=[WHOLE] * (2 * n_tp),
            out_specs=[WHOLE] * len(members),
            limit=24,
            flops=2 * rows * width,
            moved=6 * rows * width,
        )
        for d, value in zip(members, totals):
            backs[d] = shift(value, -d) if d else value

    part_send = call(
        functools.partial(parts_kernel, experts, len(groups)),
        shape((n_ep, 1, lanes), f32),
        (at, *parts[0], *parts[1]),
        in_specs=[SCALARS] + [WHOLE] * (2 * len(groups)),
        out_specs=WHOLE,
        flops=6 * n_ep * experts * lanes,
    )
    part_got = lax.all_to_all(part_send, "ep", split_axis=0, concat_axis=0, tiled=True)
    part_got = jnp.sum(part_got.reshape(experts, MEMBERS, lanes), axis=1)
    gate_back = [part_got] + [turn(part_got, k) for k in range(1, n_tp)]
    gate_grad, change, router_send = call(
        functools.partial(router_kernel, experts, cap, n_tp),
        [
            shape((TOP, ntok), f32),
            shape((experts, ntok), f32),
            shape((n_ep, experts, width // n_ep), f32),
        ],
        (at, routes.T, tokens, place, first, *gate_back),
        in_specs=[SCALARS] + [WHOLE] * (4 + n_tp),
        out_specs=[WHOLE] * 3,
        flops=6 * ntok * width * LANES,
        moved=2 * ntok * width,
    )
    router_got = lax.all_to_all(router_send, "ep", split_axis=0, concat_axis=0, tiled=True)
    router_grad = jnp.sum(router_got, axis=0).T

    n = len(toks)
    block = min(share, 512)
    per = share // block

    def home(s, tp_ref):
        return lax.rem(tp_ref[0] - s // per + n_tp, n_tp) * per + s % per

    step_of = lambda s, tp_ref: (0, s)
    still = lambda s, tp_ref: (0, 0)
    rows = sum(v.shape[0] for v in toks)
    grad_gate, grad_up = call(
        functools.partial(in_grads_kernel, n),
        [shape((width, hidden_units), f32)] * 2,
        (at_tp, *toks, *dgs, *dus),
        flops=4 * rows * width * hidden_units,
        moved=2 * rows * width + 8 * width * hidden_units,
        grid_spec=pltpu.PrefetchScalarGridSpec(
            num_scalar_prefetch=1,
            grid=(width // block,),
            in_specs=[pl.BlockSpec((v.shape[0], block), step_of) for v in toks]
            + [pl.BlockSpec(v.shape, still) for v in dgs + dus],
            out_specs=[
                pl.BlockSpec((block, hidden_units), lambda s, tp_ref: (home(s, tp_ref), 0))
            ]
            * 2,
            scratch_shapes=[pltpu.VMEM((rows, block), bf16)]
            + [pltpu.VMEM((rows, hidden_units), bf16)] * 2,
        ),
    )
    grad_down = call(
        functools.partial(out_grad_kernel, n),
        shape((hidden_units, width), f32),
        (at_tp, *cots, *scs),
        flops=2 * rows * width * hidden_units,
        moved=2 * rows * width + 4 * width * hidden_units,
        grid_spec=pltpu.PrefetchScalarGridSpec(
            num_scalar_prefetch=1,
            grid=(width // block,),
            in_specs=[pl.BlockSpec((v.shape[0], block), step_of) for v in cots]
            + [pl.BlockSpec(v.shape, still) for v in scs],
            out_specs=pl.BlockSpec((hidden_units, block), lambda s, tp_ref: (0, home(s, tp_ref))),
            scratch_shapes=[
                pltpu.VMEM((rows, block), bf16),
                pltpu.VMEM((hidden_units, rows), bf16),
            ],
        ),
    )

    token_grad = call(
        functools.partial(token_kernel, experts, share),
        shape((ntok, share), bf16),
        (at, place, change, router, *[backs[d] for d in range(experts)]),
        in_specs=[SCALARS] + [WHOLE] * (3 + experts),
        out_specs=WHOLE,
        limit=24,
        flops=2 * experts * cap * ntok * share,
        moved=6 * experts * cap * share,
    )
    return (
        token_grad, gate_grad.T, router_grad, grad_gate[None], grad_up[None], grad_down[None]
    )


def solution(mesh):
    placed = (
        P("ep", None),
        P("ep", None),
        P(),
        P("ep", None, "tp"),
        P("ep", None, "tp"),
        P("ep", "tp", None),
        P("ep", None),
    )

    return jax.shard_map(
        shards,
        mesh=mesh,
        in_specs=placed,
        out_specs=(
            P("ep", "tp"),
            P("ep", None),
            P("ep", None),
            P("ep", None, "tp"),
            P("ep", None, "tp"),
            P("ep", "tp", None),
        ),
        check_vma=False,
    )
```

time: 497 us -> 214 us (0.43)
  the two profiles are of different devices: /device:TPU:11 before, /device:TPU:0 now
where the time goes in v1:
time: 214 us; the launch traced here: 213 us
  waiting for transfers between devices  77.8 us (36%)
  Pallas kernels  58.5 us (27%)
  starting transfers between devices  49.8 us (23%)
  local copies, waits for them, and re-layouts  21.1 us (10%)
  other arithmetic  4.91 us (2%)
    pallas_call x15, Pallas kernels, call(): pl.pallas_call(body, out_shape=outs, compiler_params=pltpu.CompilerParams...  58.5 us
    ppermute x12, waiting for transfers between devices, shift(): return lax.ppermute(value, 'ep', pairs)  32.7 us
    ppermute x7, waiting for transfers between devices, turn(): lax.ppermute(value, 'tp', [(i, (i + step) % n_tp) for i in range(n_tp)])  23.3 us
    unnamed x84, local copies, waits for them, and re-layouts  20.5 us
    ppermute x12, starting transfers between devices, shift(): return lax.ppermute(value, 'ep', pairs)  16.8 us
    ppermute x14, waiting for transfers between devices, flip(): return lax.ppermute(value, 'ep', [(i, i ^ bit) for i in range(n_ep)])  13.3 us
    ppermute x14, starting transfers between devices, flip(): return lax.ppermute(value, 'ep', [(i, i ^ bit) for i in range(n_ep)])  10.5 us
    ppermute x7, starting transfers between devices, turn(): lax.ppermute(value, 'tp', [(i, (i + step) % n_tp) for i in range(n_tp)])  7.83 us
  transfers between devices with their start and end apart: 41, of which 19 were waited for; matrix products, arithmetic and copies ran while one was open for 3% of the time, Pallas kernels for 25%

profile of v1, /device:TPU:0, one launch (start us, length us, event | category | flops | bytes accessed | tf_op | source)
XLA Modules:
  0.0 213.2 jit_solution(10968855834828035917)
XLA Ops:
  1.3 2.6 %shard_map.118 = (bf16[4,80,128]{2,1,0:T(8,128)(2,1)}, bf16[80,1024]{1,0:T(8,128)(2,1)}, bf16[80,1024]{1,0:T(8,128)(2,1)}, bf16[80,1024]{1,0:T(8,128)(2,1)}, bf1...) custom-call(s32[3]{0:T(128)} %pad_add_fusion.at_ref, ...), custom_call_target="tpu_custom_call" | custom-call | flops 167772160 | bytes 1048576 | tf_op jit(solution)/shard_map/pallas_call | solution.py:30
  3.9 3.1 %collective-permute-start = (bf16[80,1024]{1,0:T(8,128)(2,1)}, bf16[80,1024]{1,0:T(8,128)(2,1)S(1)}, u32[]{:S(2)}, u32[]{:S(2)}) collective-permute-start(bf16[80,1024]{1,0:T(8,128)(2,1)} %get-tuple-element.59), channel_id=1, source_target_pairs={{0,8},{2,10},{4,12},{6,14},{8,16},{10,18},{12,20},{14,22},{16,24},... | collective-permute-start | bytes 491528 | tf_op jit(solution)/shard_map/ppermute | solution.py:306
  7.0 2.1 collective-permute-start.1
  9.0 3.8 %collective-permute-start.6 = (bf16[80,1024]{1,0:T(8,128)(2,1)}, bf16[80,1024]{1,0:T(8,128)(2,1)S(1)}, u32[]{:S(2)}, u32[]{:S(2)}) collective-permute-start(bf16[80,1024]{1,0:T(8,128)(2,1)} %get-tuple-element.63), channel_id=1, source_target_pairs={{0,24},{2,26},{4,28},{6,30},{8,0},{10,2},{12,4},{14,6},{16,8},{18,... | collective-permute-start | bytes 491528 | tf_op jit(solution)/shard_map/ppermute | solution.py:306
  12.9 0.9 constant_dynamic-update-slice_fusion.2
  14.3 3.6 %collective-permute-done.1 = bf16[80,1024]{1,0:T(8,128)(2,1)S(1)} collective-permute-done((bf16[80,1024]{1,0:T(8,128)(2,1)}, bf16[80,1024]{1,0:T(8,128)(2,1)S(1)}, u32[]{:S(2)}, u32[]{:S(2)}) %collective-permute-start.1) | collective-permute-done | bytes 163872 | tf_op jit(solution)/shard_map/ppermute | solution.py:306
  17.9 1.8 collective-permute-start.3
  19.7 0.9 constant_dynamic-update-slice_fusion.5
  21.4 2.0 collective-permute-done.6
  23.4 1.6 collective-permute-start.7
  25.5 3.5 %collective-permute-done.3 = bf16[240,1024]{1,0:T(8,128)(2,1)S(1)} collective-permute-done((bf16[240,1024]{1,0:T(8,128)(2,1)S(1)}, bf16[240,1024]{1,0:T(8,128)(2,1)S(1)}, u32[]{:S(2)}, u32[]{:S(2)}) %collective-permute-start.3) | collective-permute-done | bytes 491552 | tf_op jit(solution)/shard_map/ppermute | solution.py:302
  29.0 1.6 collective-permute-start.4
  30.6 1.7 collective-permute-start.8
  32.3 5.2 %collective-permute-done.7 = bf16[240,1024]{1,0:T(8,128)(2,1)S(1)} collective-permute-done((bf16[240,1024]{1,0:T(8,128)(2,1)S(1)}, bf16[240,1024]{1,0:T(8,128)(2,1)S(1)}, u32[]{:S(2)}, u32[]{:S(2)}) %collective-permute-start.7) | collective-permute-done | bytes 491552 | tf_op jit(solution)/shard_map/ppermute | solution.py:309
  37.6 1.5 collective-permute-start.9
  39.0 9.0 %collective-permute-done.2 = bf16[240,1024]{1,0:T(8,128)(2,1)S(1)} collective-permute-done((bf16[240,1024]{1,0:T(8,128)(2,1)S(1)}, bf16[240,1024]{1,0:T(8,128)(2,1)S(1)}, u32[]{:S(2)}, u32[]{:S(2)}) %collective-permute-start.2) | collective-permute-done | bytes 491552 | tf_op jit(solution)/shard_map/ppermute | solution.py:309
  48.1 9.0 %collective-permute-done.4 = bf16[240,1024]{1,0:T(8,128)(2,1)S(1)} collective-permute-done((bf16[240,1024]{1,0:T(8,128)(2,1)S(1)}, bf16[240,1024]{1,0:T(8,128)(2,1)S(1)}, u32[]{:S(2)}, u32[]{:S(2)}) %collective-permute-start.4) | collective-permute-done | bytes 491552 | tf_op jit(solution)/shard_map/ppermute | solution.py:309
  57.1 1.4 maximum_maximum_fusion.tok_ref.refs_0_
  58.6 1.4 maximum_maximum_fusion.1.cot_ref.refs_0_
  60.5 1.0 collective-permute-start.18
  61.5 1.9 collective-permute-start.14
  63.4 12.1 %collective-permute-done.18 = bf16[80,1024]{1,0:T(8,128)(2,1)S(1)} collective-permute-done((bf16[80,1024]{1,0:T(8,128)(2,1)S(1)}, bf16[80,1024]{1,0:T(8,128)(2,1)S(1)}, u32[]{:S(2)}, u32[]{:S(2)}) %collective-permute-start.18) | collective-permute-done | bytes 163872 | tf_op jit(solution)/shard_map/ppermute | solution.py:306
  75.5 1.5 collective-permute-start.19
  77.0 2.1 shard_map.119
  79.1 5.5 %collective-permute-done.10 = f32[1,128]{1,0:T(1,128)S(1)} collective-permute-done((f32[1,128]{1,0:T(1,128)}, f32[1,128]{1,0:T(1,128)S(1)}, u32[]{:S(2)}, u32[]{:S(2)}) %collective-permute-start.10) | collective-permute-done | bytes 544 | tf_op jit(solution)/shard_map/ppermute | solution.py:306
  84.6 4.6 %collective-permute-done.11 = f32[1,128]{1,0:T(1,128)S(1)} collective-permute-done((f32[1,128]{1,0:T(1,128)}, f32[1,128]{1,0:T(1,128)S(1)}, u32[]{:S(2)}, u32[]{:S(2)}) %collective-permute-start.11) | collective-permute-done | bytes 544 | tf_op jit(solution)/shard_map/ppermute | solution.py:306
  89.2 3.7 %collective-permute-done.12 = f32[1,128]{1,0:T(1,128)S(1)} collective-permute-done((f32[1,128]{1,0:T(1,128)}, f32[1,128]{1,0:T(1,128)S(1)}, u32[]{:S(2)}, u32[]{:S(2)}) %collective-permute-start.12) | collective-permute-done | bytes 544 | tf_op jit(solution)/shard_map/ppermute | solution.py:306
  93.6 1.5 collective-permute-start.13
  95.6 1.6 collective-permute-done.13
  97.2 1.5 collective-permute-start.20
  100.4 2.1 collective-permute-done.20
  103.0 1.2 collective-permute-done.21
  104.9 1.7 copy-done.1
  106.6 1.6 copy-done.4
  108.2 9.6 %shard_map.122 = (bf16[480,512]{1,0:T(8,128)(2,1)S(1)}, bf16[480,512]{1,0:T(8,128)(2,1)S(1)}, bf16[480,512]{1,0:T(8,128)(2,1)S(1)}, bf16[480,2048]{1,0:T(8,128)(2,1)}, f32[8,128]{1,0:T(8,128)S(1)}) custom-call(s32[1]{0:T(128)} %bitcast.1.tp_ref, bf16[480,2048]{1,0:T(8,128)(2,1)} %collective-permute-done.22.tok_ref.refs_1_, ...), custom_call_target="tpu_custom_call" | custom-call | flops 5033164800 | bytes 12189696 | tf_op jit(solution)/shard_map/pallas_call | solution.py:30
  117.8 0.8 copy-done.32
  119.4 4.4 %collective-permute-done.25.tok_ref.refs_3_ = bf16[160,2048]{1,0:T(8,128)(2,1)S(1)} collective-permute-done((bf16[160,2048]{1,0:T(8,128)(2,1)S(1)}, bf16[160,2048]{1,0:T(8,128)(2,1)S(1)}, u32[]{:S(2)}, u32[]{:S(2)}) %collective-permute-start.25) | collective-permute-done | bytes 655392 | tf_op jit(solution)/shard_map/ppermute | solution.py:302
  123.8 3.1 %shard_map.123 = (bf16[160,512]{1,0:T(8,128)(2,1)S(1)}, bf16[160,512]{1,0:T(8,128)(2,1)S(1)}, bf16[160,512]{1,0:T(8,128)(2,1)S(1)}, bf16[160,2048]{1,0:T(8,128)(2,1)S(1)}, f32[8,128]{1,0:T(8,128)S(1)}) custom-call(s32[1]{0:T(128)} %bitcast.1.tp_ref, bf16[160,2048]{1,0:T(8,128)(2,1)S(1)} %collective-permute-done.25.tok_ref.refs_3_, ...), custom_call_target="tpu_custom_call" | custom-call | flops 1677721600 | bytes 8257536 | tf_op jit(solution)/shard_map/pallas_call | solution.py:30
  129.3 3.1 %shard_map.121 = (bf16[160,512]{1,0:T(8,128)(2,1)S(1)}, bf16[160,512]{1,0:T(8,128)(2,1)S(1)}, bf16[160,512]{1,0:T(8,128)(2,1)S(1)}, bf16[160,2048]{1,0:T(8,128)(2,1)S(1)}, f32[8,128]{1,0:T(8,128)S(1)}) custom-call(s32[1]{0:T(128)} %bitcast.1.tp_ref, bf16[160,2048]{1,0:T(8,128)(2,1)S(1)} %maximum_maximum_fusion.2.tok_ref.refs_2_, ...), custom_call_target="tpu_custom_call" | custom-call | flops 1677721600 | bytes 8257536 | tf_op jit(solution)/shard_map/pallas_call | solution.py:30
  132.3 0.8 copy-done.12
  135.8 0.8 copy-done.35
  136.6 2.2 %shard_map.128 = (bf16[80,1024]{1,0:T(8,128)(2,1)}, bf16[80,1024]{1,0:T(8,128)(2,1)}, bf16[80,1024]{1,0:T(8,128)(2,1)}, bf16[80,1024]{1,0:T(8,128)(2,1)}) custom-call(bf16[160,2048]{1,0:T(8,128)(2,1)} %copy-done.12, bf16[160,2048]{1,0:T(8,128)(2,1)} %copy-done.35), custom_call_target="tpu_custom_call" | custom-call | flops 327680 | bytes 1966080 | tf_op jit(solution)/shard_map/pallas_call | solution.py:30
  138.8 1.5 collective-permute-start.34
  140.3 1.5 collective-permute-start.35
  142.3 1.6 copy-done.3
  143.9 1.6 copy-done.6
  145.5 8.4 %shard_map.120 = (bf16[480,512]{1,0:T(8,128)(2,1)S(1)}, bf16[480,512]{1,0:T(8,128)(2,1)S(1)}, bf16[480,512]{1,0:T(8,128)(2,1)S(1)}, bf16[480,2048]{1,0:T(8,128)(2,1)S(1)}, f32[8,128]{1,0:T(8,128)S(1)}) custom-call(s32[1]{0:T(128)} %bitcast.1.tp_ref, bf16[480,2048]{1,0:T(8,128)(2,1)} %maximum_maximum_fusion.tok_ref.refs_0_, ...), custom_call_target="tpu_custom_call" | custom-call | flops 5033164800 | bytes 12189696 | tf_op jit(solution)/shard_map/pallas_call | solution.py:30
  153.9 1.3 copy-done.10
  156.5 0.8 copy-done.33
  157.3 0.8 copy-done.34
  158.1 1.5 shard_map.124
  159.6 4.1 %all-to-all-start = ((f32[16,1,128]{2,1,0:T(1,128)}), f32[16,1,128]{2,1,0:T(1,128)S(1)}, u32[]{:S(2)}, u32[]{:S(2)}) async-start(f32[16,1,128]{2,1,0:T(1,128)} %shard_map.124), calls=%async_computation | async-start | bytes 16384 | tf_op jit(solution)/shard_map/all_to_all | solution.py:455
  163.9 2.9 %collective-permute-start.37 = (bf16[80,1024]{1,0:T(8,128)(2,1)S(1)}, bf16[80,1024]{1,0:T(8,128)(2,1)S(1)}, u32[]{:S(2)}, u32[]{:S(2)}) collective-permute-start(bf16[80,1024]{1,0:T(8,128)(2,1)S(1)} %shard_map.129), channel_id=1, source_target_pairs={{0,16},{2,18},{4,20},{6,22},{8,24},{10,26},{12,28},{14,30},{16,0},... | collective-permute-start | bytes 491528 | tf_op jit(solution)/shard_map/ppermute | solution.py:306
  166.8 3.5 %all-to-all-done = f32[16,1,128]{2,1,0:T(1,128)S(1)} async-done(((f32[16,1,128]{2,1,0:T(1,128)}), f32[16,1,128]{2,1,0:T(1,128)S(1)}, u32[]{:S(2)}, u32[]{:S(2)}) %all-to-all-start) | async-done | bytes 8224 | tf_op jit(solution)/shard_map/all_to_all | solution.py:455
  170.3 1.6 collective-permute-start.27
  171.9 3.5 %shard_map.126 = (bf16[240,1024]{1,0:T(8,128)(2,1)}, bf16[240,1024]{1,0:T(8,128)(2,1)}, bf16[240,1024]{1,0:T(8,128)(2,1)}, bf16[240,1024]{1,0:T(8,128)(2,1)}) custom-call(bf16[480,2048]{1,0:T(8,128)(2,1)} %copy-done.10, bf16[480,2048]{1,0:T(8,128)(2,1)} %collective-permute-done.28.refs_1_), custom_call_target="tpu_custom_call" | custom-call | flops 983040 | bytes 5898240 | tf_op jit(solution)/shard_map/pallas_call | solution.py:30
  176.2 2.7 %collective-permute-start.31 = (bf16[240,1024]{1,0:T(8,128)(2,1)}, bf16[240,1024]{1,0:T(8,128)(2,1)S(1)}, u32[]{:S(2)}, u32[]{:S(2)}) collective-permute-start(bf16[240,1024]{1,0:T(8,128)(2,1)} %get-tuple-element.80), channel_id=1, source_target_pairs={{0,5},{1,4},{2,7},{3,6},{4,1},{5,0},{6,3},{7,2},{8,13},{9,12},{10,... | collective-permute-start | bytes 1474568 | tf_op jit(solution)/shard_map/ppermute | solution.py:317
  178.9 9.9 %shard_map.131 = (f32[2048,512]{1,0:T(8,128)}, f32[2048,512]{1,0:T(8,128)}) custom-call(s32[1]{0:T(128)} %bitcast.1.tp_ref, bf16[480,2048]{1,0:T(8,128)(2,1)} %maximum_maximum_fusion.tok_ref.refs_0_, bf16[480,2048]{1,0:T(8,128)(2,1)} %collective-permute-done.22.tok_ref.refs_1_, bf16[160,2048]{1,0:T(8,128)(2,1)} %copy-done.8, bf16[160,2048]{1,0:T(8,128)(2,1)} %copy-done.11, ...), custom_call_target="tpu_custom_call" | custom-call | flops 5368709120 | bytes 13631488 | tf_op jit(solution)/shard_map/pallas_call | solution.py:30
  189.4 2.2 %shard_map.125 = (f32[2,128]{1,0:T(2,128)}, f32[4,128]{1,0:T(4,128)}, f32[16,4,128]{2,1,0:T(4,128)}) custom-call(s32[3]{0:T(128)} %pad_add_fusion.at_ref, s32[2,128]{1,0:T(2,128)} %bitcast.32, bf16[128,2048]{1,0:T(8,128)(2,1)} %tok_ref.5, bf16[4,80,128]{2,1,0:T(8,128)(2,1)} %get-tuple-element.56.place_ref, f32[1,128]{1,0:T(1,128)} %get-tuple-element.57.first_ref, ...), custom_call_target="tpu_custom_call" | custom-call | flops 201326592 | bytes 524288 | tf_op jit(solution)/shard_map/pallas_call | solution.py:30
  191.6 3.5 %all-to-all-start.1 = ((f32[16,4,128]{2,1,0:T(4,128)}), f32[16,4,128]{2,1,0:T(4,128)S(1)}, u32[]{:S(2)}, u32[]{:S(2)}) async-start(f32[16,4,128]{2,1,0:T(4,128)} %get-tuple-element.91), calls=%async_computation.1 | async-start | bytes 65536 | tf_op jit(solution)/shard_map/all_to_all | solution.py:471
  195.1 5.0 %collective-permute-done.31.refs_3_ = bf16[240,1024]{1,0:T(8,128)(2,1)S(1)} collective-permute-done((bf16[240,1024]{1,0:T(8,128)(2,1)}, bf16[240,1024]{1,0:T(8,128)(2,1)S(1)}, u32[]{:S(2)}, u32[]{:S(2)}) %collective-permute-start.31) | collective-permute-done | bytes 491552 | tf_op jit(solution)/shard_map/ppermute | solution.py:317
  200.8 1.6 collective-permute-start.38
  202.5 8.2 %shard_map.132 = f32[512,2048]{1,0:T(8,128)} custom-call(s32[1]{0:T(128)} %bitcast.1.tp_ref, bf16[480,2048]{1,0:T(8,128)(2,1)} %maximum_maximum_fusion.1.cot_ref.refs_0_, bf16[480,2048]{1,0:T(8,128)(2,1)} %collective-permute-done.23.cot_ref.refs_1_, bf16[160,2048]{1,0:T(8,128)(2,1)} %copy-done.7, bf16[160,2048]{1,0:T(8,128)(2,1)} %copy-done.9, ...), custom_call_target="tpu_custom_call" | custom-call | flops 2684354560 | bytes 9437184 | tf_op jit(solution)/shard_map/pallas_call | solution.py:30
  211.3 1.9 shard_map.130
  (128 shorter events, 17.6 us)
Async XLA Ops:
  3.9 10.4 %collective-permute-start = (bf16[80,1024]{1,0:T(8,128)(2,1)}, bf16[80,1024]{1,0:T(8,128)(2,1)S(1)}, u32[]{:S(2)}, u32[]{:S(2)}) collective-permute-start(bf16[80,1024]{1,0:T(8,128)(2,1)} %get-tuple-element.59), channel_id=1, source_target_pairs={{0,8},{2,10},{4,12},{6,14},{8,16},{10,18},{12,20},{14,22},{16,24},... | collective-permute-start | bytes 491528 | tf_op jit(solution)/shard_map/ppermute | solution.py:306
  7.0 10.9 %collective-permute-start.1 = (bf16[80,1024]{1,0:T(8,128)(2,1)}, bf16[80,1024]{1,0:T(8,128)(2,1)S(1)}, u32[]{:S(2)}, u32[]{:S(2)}) collective-permute-start(bf16[80,1024]{1,0:T(8,128)(2,1)} %get-tuple-element.60), channel_id=1, source_target_pairs={{0,24},{2,26},{4,28},{6,30},{8,0},{10,2},{12,4},{14,6},{16,8},{18,... | collective-permute-start | bytes 491528 | tf_op jit(solution)/shard_map/ppermute | solution.py:306
  9.0 12.3 %collective-permute-start.5 = (bf16[80,1024]{1,0:T(8,128)(2,1)}, bf16[80,1024]{1,0:T(8,128)(2,1)S(1)}, u32[]{:S(2)}, u32[]{:S(2)}) collective-permute-start(bf16[80,1024]{1,0:T(8,128)(2,1)} %get-tuple-element.62), channel_id=1, source_target_pairs={{0,8},{2,10},{4,12},{6,14},{8,16},{10,18},{12,20},{14,22},{16,24},... | collective-permute-start | bytes 491528 | tf_op jit(solution)/shard_map/ppermute | solution.py:306
  9.0 14.3 %collective-permute-start.6 = (bf16[80,1024]{1,0:T(8,128)(2,1)}, bf16[80,1024]{1,0:T(8,128)(2,1)S(1)}, u32[]{:S(2)}, u32[]{:S(2)}) collective-permute-start(bf16[80,1024]{1,0:T(8,128)(2,1)} %get-tuple-element.63), channel_id=1, source_target_pairs={{0,24},{2,26},{4,28},{6,30},{8,0},{10,2},{12,4},{14,6},{16,8},{18,... | collective-permute-start | bytes 491528 | tf_op jit(solution)/shard_map/ppermute | solution.py:306
  17.9 11.1 %collective-permute-start.3 = (bf16[240,1024]{1,0:T(8,128)(2,1)S(1)}, bf16[240,1024]{1,0:T(8,128)(2,1)S(1)}, u32[]{:S(2)}, u32[]{:S(2)}) collective-permute-start(bf16[240,1024]{1,0:T(8,128)(2,1)S(1)} %constant_dynamic-update-slice_fusion), channel_id=1, source_target_pairs={{0,4},{2,6},{4,0},{6,2},{8,12},{10,14},{12,8},{14,10},{16,20},{18,... | collective-permute-start | bytes 1474568 | tf_op jit(solution)/shard_map/ppermute | solution.py:302
  23.4 14.2 %collective-permute-start.7 = (bf16[240,1024]{1,0:T(8,128)(2,1)S(1)}, bf16[240,1024]{1,0:T(8,128)(2,1)S(1)}, u32[]{:S(2)}, u32[]{:S(2)}) collective-permute-start(bf16[240,1024]{1,0:T(8,128)(2,1)S(1)} %constant_dynamic-update-slice_fusion.3), channel_id=1, source_target_pairs={{0,1},{1,0},{2,3},{3,2},{4,5},{5,4},{6,7},{7,6},{8,9},{9,8},{10,11... | collective-permute-start | bytes 1474568 | tf_op jit(solution)/shard_map/ppermute | solution.py:309
  25.0 23.1 %collective-permute-start.2 = (bf16[240,1024]{1,0:T(8,128)(2,1)S(1)}, bf16[240,1024]{1,0:T(8,128)(2,1)S(1)}, u32[]{:S(2)}, u32[]{:S(2)}) collective-permute-start(bf16[240,1024]{1,0:T(8,128)(2,1)S(1)} %constant_dynamic-update-slice_fusion), channel_id=1, source_target_pairs={{0,1},{1,0},{2,3},{3,2},{4,5},{5,4},{6,7},{7,6},{8,9},{9,8},{10,11... | collective-permute-start | bytes 1474568 | tf_op jit(solution)/shard_map/ppermute | solution.py:309
  29.0 28.1 %collective-permute-start.4 = (bf16[240,1024]{1,0:T(8,128)(2,1)S(1)}, bf16[240,1024]{1,0:T(8,128)(2,1)S(1)}, u32[]{:S(2)}, u32[]{:S(2)}) collective-permute-start(bf16[240,1024]{1,0:T(8,128)(2,1)S(1)} %collective-permute-done.3), channel_id=1, source_target_pairs={{0,1},{1,0},{2,3},{3,2},{4,5},{5,4},{6,7},{7,6},{8,9},{9,8},{10,11... | collective-permute-start | bytes 1474568 | tf_op jit(solution)/shard_map/ppermute | solution.py:309
  30.6 27.9 %collective-permute-start.8 = (bf16[240,1024]{1,0:T(8,128)(2,1)S(1)}, bf16[240,1024]{1,0:T(8,128)(2,1)S(1)}, u32[]{:S(2)}, u32[]{:S(2)}) collective-permute-start(bf16[240,1024]{1,0:T(8,128)(2,1)S(1)} %constant_dynamic-update-slice_fusion.3), channel_id=1, source_target_pairs={{0,4},{2,6},{4,0},{6,2},{8,12},{10,14},{12,8},{14,10},{16,20},{18,... | collective-permute-start | bytes 1474568 | tf_op jit(solution)/shard_map/ppermute | solution.py:302
  37.6 21.0 %collective-permute-start.9 = (bf16[240,1024]{1,0:T(8,128)(2,1)S(1)}, bf16[240,1024]{1,0:T(8,128)(2,1)S(1)}, u32[]{:S(2)}, u32[]{:S(2)}) collective-permute-start(bf16[240,1024]{1,0:T(8,128)(2,1)S(1)} %collective-permute-done.7), channel_id=1, source_target_pairs={{0,4},{2,6},{4,0},{6,2},{8,12},{10,14},{12,8},{14,10},{16,20},{18,... | collective-permute-start | bytes 1474568 | tf_op jit(solution)/shard_map/ppermute | solution.py:302
  58.5 2.0 copy-start.38
  58.6 3.0 %copy-start.37 = (bf16[80,1024]{1,0:T(8,128)(2,1)S(1)}, bf16[80,1024]{1,0:T(8,128)(2,1)}, u32[]{:S(2)}) copy-start(bf16[80,1024]{1,0:T(8,128)(2,1)} %get-tuple-element.69) | copy-start | bytes 491524
  58.6 46.3 %collective-permute-start.22 = (bf16[480,2048]{1,0:T(8,128)(2,1)}, bf16[480,2048]{1,0:T(8,128)(2,1)}, u32[]{:S(2)}, u32[]{:S(2)}) collective-permute-start(bf16[480,2048]{1,0:T(8,128)(2,1)} %maximum_maximum_fusion.tok_ref.refs_0_), channel_id=1, source_target_pairs={{0,2},{2,0},{4,6},{6,4},{8,10},{10,8},{12,14},{14,12},{16,18},{18,... | collective-permute-start | bytes 5898248 | tf_op jit(solution)/shard_map/ppermute | solution.py:302
  58.6 46.3 %copy-start = (bf16[1,2048,512]{2,1,0:T(8,128)(2,1)S(1)}, bf16[1,2048,512]{2,1,0:T(8,128)(2,1)}, u32[]{:S(2)}) copy-start(bf16[1,2048,512]{2,1,0:T(8,128)(2,1)} %param.10) | copy-start | bytes 6291460
  60.0 44.9 %collective-permute-start.23 = (bf16[480,2048]{1,0:T(8,128)(2,1)}, bf16[480,2048]{1,0:T(8,128)(2,1)}, u32[]{:S(2)}, u32[]{:S(2)}) collective-permute-start(bf16[480,2048]{1,0:T(8,128)(2,1)} %maximum_maximum_fusion.1.cot_ref.refs_0_), channel_id=1, source_target_pairs={{0,2},{2,0},{4,6},{6,4},{8,10},{10,8},{12,14},{14,12},{16,18},{18,... | collective-permute-start | bytes 5898248 | tf_op jit(solution)/shard_map/ppermute | solution.py:302
  60.5 15.0 %collective-permute-start.18 = (bf16[80,1024]{1,0:T(8,128)(2,1)S(1)}, bf16[80,1024]{1,0:T(8,128)(2,1)S(1)}, u32[]{:S(2)}, u32[]{:S(2)}) collective-permute-start(bf16[80,1024]{1,0:T(8,128)(2,1)S(1)} %copy-done.38), channel_id=1, source_target_pairs={{0,16},{2,18},{4,20},{6,22},{8,24},{10,26},{12,28},{14,30},{16,0},... | collective-permute-start | bytes 491528 | tf_op jit(solution)/shard_map/ppermute | solution.py:306
  61.5 33.5 %collective-permute-start.14 = (bf16[80,1024]{1,0:T(8,128)(2,1)S(1)}, bf16[80,1024]{1,0:T(8,128)(2,1)S(1)}, u32[]{:S(2)}, u32[]{:S(2)}) collective-permute-start(bf16[80,1024]{1,0:T(8,128)(2,1)S(1)} %copy-done.37), channel_id=1, source_target_pairs={{0,16},{2,18},{4,20},{6,22},{8,24},{10,26},{12,28},{14,30},{16,0},... | collective-permute-start | bytes 491528 | tf_op jit(solution)/shard_map/ppermute | solution.py:306
  75.5 23.2 %collective-permute-start.19 = (bf16[80,1024]{1,0:T(8,128)(2,1)S(1)}, bf16[80,1024]{1,0:T(8,128)(2,1)S(1)}, u32[]{:S(2)}, u32[]{:S(2)}) collective-permute-start(bf16[80,1024]{1,0:T(8,128)(2,1)S(1)} %collective-permute-done.18), channel_id=1, source_target_pairs={{0,1},{1,0},{2,3},{3,2},{4,5},{5,4},{6,7},{7,6},{8,9},{9,8},{10,11... | collective-permute-start | bytes 491528 | tf_op jit(solution)/shard_map/ppermute | solution.py:309
  79.1 5.5 %collective-permute-start.10 = (f32[1,128]{1,0:T(1,128)}, f32[1,128]{1,0:T(1,128)S(1)}, u32[]{:S(2)}, u32[]{:S(2)}) collective-permute-start(f32[1,128]{1,0:T(1,128)} %get-tuple-element.65), channel_id=1, source_target_pairs={{0,8},{2,10},{4,12},{6,14},{8,16},{10,18},{12,20},{14,22},{16,24},... | collective-permute-start | bytes 1544 | tf_op jit(solution)/shard_map/ppermute | solution.py:306
  84.6 4.6 %collective-permute-start.11 = (f32[1,128]{1,0:T(1,128)}, f32[1,128]{1,0:T(1,128)S(1)}, u32[]{:S(2)}, u32[]{:S(2)}) collective-permute-start(f32[1,128]{1,0:T(1,128)} %get-tuple-element.66), channel_id=1, source_target_pairs={{0,16},{2,18},{4,20},{6,22},{8,24},{10,26},{12,28},{14,30},{16,0},... | collective-permute-start | bytes 1544 | tf_op jit(solution)/shard_map/ppermute | solution.py:306
  89.2 3.7 %collective-permute-start.12 = (f32[1,128]{1,0:T(1,128)}, f32[1,128]{1,0:T(1,128)S(1)}, u32[]{:S(2)}, u32[]{:S(2)}) collective-permute-start(f32[1,128]{1,0:T(1,128)} %get-tuple-element.67), channel_id=1, source_target_pairs={{0,24},{2,26},{4,28},{6,30},{8,0},{10,2},{12,4},{14,6},{16,8},{18,... | collective-permute-start | bytes 1544 | tf_op jit(solution)/shard_map/ppermute | solution.py:306
  93.6 3.6 %collective-permute-start.13 = (f32[4,128]{1,0:T(4,128)S(1)}, f32[4,128]{1,0:T(4,128)S(1)}, u32[]{:S(2)}, u32[]{:S(2)}) collective-permute-start(f32[4,128]{1,0:T(4,128)S(1)} %pad_maximum_fusion), channel_id=1, source_target_pairs={{0,4},{2,6},{4,0},{6,2},{8,12},{10,14},{12,8},{14,10},{16,20},{18,... | collective-permute-start | bytes 6152 | tf_op jit(solution)/shard_map/ppermute | solution.py:302
  95.1 5.3 %collective-permute-start.16 = (bf16[80,1024]{1,0:T(8,128)(2,1)S(1)}, bf16[80,1024]{1,0:T(8,128)(2,1)S(1)}, u32[]{:S(2)}, u32[]{:S(2)}) collective-permute-start(bf16[80,1024]{1,0:T(8,128)(2,1)S(1)} %collective-permute-done.14), channel_id=1, source_target_pairs={{0,4},{2,6},{4,0},{6,2},{8,12},{10,14},{12,8},{14,10},{16,20},{18,... | collective-permute-start | bytes 491528 | tf_op jit(solution)/shard_map/ppermute | solution.py:302
  97.2 5.3 %collective-permute-start.20 = (bf16[80,1024]{1,0:T(8,128)(2,1)S(1)}, bf16[80,1024]{1,0:T(8,128)(2,1)S(1)}, u32[]{:S(2)}, u32[]{:S(2)}) collective-permute-start(bf16[80,1024]{1,0:T(8,128)(2,1)S(1)} %collective-permute-done.18), channel_id=1, source_target_pairs={{0,4},{2,6},{4,0},{6,2},{8,12},{10,14},{12,8},{14,10},{16,20},{18,... | collective-permute-start | bytes 491528 | tf_op jit(solution)/shard_map/ppermute | solution.py:302
  98.7 5.6 %collective-permute-start.21 = (bf16[80,1024]{1,0:T(8,128)(2,1)S(1)}, bf16[80,1024]{1,0:T(8,128)(2,1)S(1)}, u32[]{:S(2)}, u32[]{:S(2)}) collective-permute-start(bf16[80,1024]{1,0:T(8,128)(2,1)S(1)} %collective-permute-done.19), channel_id=1, source_target_pairs={{0,4},{2,6},{4,0},{6,2},{8,12},{10,14},{12,8},{14,10},{16,20},{18,... | collective-permute-start | bytes 491528 | tf_op jit(solution)/shard_map/ppermute | solution.py:302
  100.4 4.4 %collective-permute-start.24 = (f32[8,128]{1,0:T(8,128)S(1)}, f32[8,128]{1,0:T(8,128)S(1)}, u32[]{:S(2)}, u32[]{:S(2)}) collective-permute-start(f32[8,128]{1,0:T(8,128)S(1)} %concatenate.58.gate_ref), channel_id=1, source_target_pairs={{0,2},{2,0},{4,6},{6,4},{8,10},{10,8},{12,14},{14,12},{16,18},{18,... | collective-permute-start | bytes 12296 | tf_op jit(solution)/shard_map/ppermute | solution.py:302
  102.5 16.5 %collective-permute-start.15 = (bf16[80,1024]{1,0:T(8,128)(2,1)S(1)}, bf16[80,1024]{1,0:T(8,128)(2,1)S(1)}, u32[]{:S(2)}, u32[]{:S(2)}) collective-permute-start(bf16[80,1024]{1,0:T(8,128)(2,1)S(1)} %collective-permute-done.14), channel_id=1, source_target_pairs={{0,1},{1,0},{2,3},{3,2},{4,5},{5,4},{6,7},{7,6},{8,9},{9,8},{10,11... | collective-permute-start | bytes 491528 | tf_op jit(solution)/shard_map/ppermute | solution.py:309
  104.2 14.8 %collective-permute-start.17 = (bf16[80,1024]{1,0:T(8,128)(2,1)S(1)}, bf16[80,1024]{1,0:T(8,128)(2,1)S(1)}, u32[]{:S(2)}, u32[]{:S(2)}) collective-permute-start(bf16[80,1024]{1,0:T(8,128)(2,1)S(1)} %collective-permute-done.16), channel_id=1, source_target_pairs={{0,1},{1,0},{2,3},{3,2},{4,5},{5,4},{6,7},{7,6},{8,9},{9,8},{10,11... | collective-permute-start | bytes 491528 | tf_op jit(solution)/shard_map/ppermute | solution.py:309
  104.8 24.5 %copy-start.7 = (bf16[160,2048]{1,0:T(8,128)(2,1)}, bf16[160,2048]{1,0:T(8,128)(2,1)S(1)}, u32[]{:S(2)}) copy-start(bf16[160,2048]{1,0:T(8,128)(2,1)S(1)} %maximum_maximum_fusion.3.cot_ref.refs_2_) | copy-start | bytes 1966084
  104.8 14.5 %collective-permute-start.26 = (bf16[160,2048]{1,0:T(8,128)(2,1)S(1)}, bf16[160,2048]{1,0:T(8,128)(2,1)S(1)}, u32[]{:S(2)}, u32[]{:S(2)}) collective-permute-start(bf16[160,2048]{1,0:T(8,128)(2,1)S(1)} %maximum_maximum_fusion.3.cot_ref.refs_2_), channel_id=1, source_target_pairs={{0,2},{2,0},{4,6},{6,4},{8,10},{10,8},{12,14},{14,12},{16,18},{18,... | collective-permute-start | bytes 1966088 | tf_op jit(solution)/shard_map/ppermute | solution.py:302
  104.9 1.7 copy-start.1
  106.6 1.6 copy-start.4
  108.2 15.5 %copy-start.5 = (bf16[1,512,2048]{2,1,0:T(8,128)(2,1)S(1)}, bf16[1,512,2048]{2,1,0:T(8,128)(2,1)}, u32[]{:S(2)}) copy-start(bf16[1,512,2048]{2,1,0:T(8,128)(2,1)} %param.12) | copy-start | bytes 6291460
  118.6 8.2 %copy-start.14 = (bf16[480,512]{1,0:T(8,128)(2,1)}, bf16[480,512]{1,0:T(8,128)(2,1)S(1)}, u32[]{:S(2)}) copy-start(bf16[480,512]{1,0:T(8,128)(2,1)S(1)} %get-tuple-element.103.refs_5_) | copy-start | bytes 1474564
  118.6 8.2 %copy-start.22 = (f32[8,128]{1,0:T(8,128)}, f32[8,128]{1,0:T(8,128)S(1)}, u32[]{:S(2)}) copy-start(f32[8,128]{1,0:T(8,128)S(1)} %get-tuple-element.72.refs_2_) | copy-start | bytes 12292
  118.6 53.3 %collective-permute-start.28 = (bf16[480,2048]{1,0:T(8,128)(2,1)}, bf16[480,2048]{1,0:T(8,128)(2,1)}, u32[]{:S(2)}, u32[]{:S(2)}) collective-permute-start(bf16[480,2048]{1,0:T(8,128)(2,1)} %get-tuple-element.76), channel_id=1, source_target_pairs={{0,2},{2,0},{4,6},{6,4},{8,10},{10,8},{12,14},{14,12},{16,18},{18,... | collective-permute-start | bytes 5898248 | tf_op jit(solution)/shard_map/ppermute | solution.py:302
  119.0 10.2 %copy-start.8 = (bf16[160,2048]{1,0:T(8,128)(2,1)}, bf16[160,2048]{1,0:T(8,128)(2,1)S(1)}, u32[]{:S(2)}) copy-start(bf16[160,2048]{1,0:T(8,128)(2,1)S(1)} %maximum_maximum_fusion.2.tok_ref.refs_2_) | copy-start | bytes 1966084
  119.1 10.2 %copy-start.2 = (bf16[1,2048,512]{2,1,0:T(8,128)(2,1)S(1)}, bf16[1,2048,512]{2,1,0:T(8,128)(2,1)}, u32[]{:S(2)}) copy-start(bf16[1,2048,512]{2,1,0:T(8,128)(2,1)} %param.11) | copy-start | bytes 6291460
  119.1 4.7 %collective-permute-start.25 = (bf16[160,2048]{1,0:T(8,128)(2,1)S(1)}, bf16[160,2048]{1,0:T(8,128)(2,1)S(1)}, u32[]{:S(2)}, u32[]{:S(2)}) collective-permute-start(bf16[160,2048]{1,0:T(8,128)(2,1)S(1)} %maximum_maximum_fusion.2.tok_ref.refs_2_), channel_id=1, source_target_pairs={{0,2},{2,0},{4,6},{6,4},{8,10},{10,8},{12,14},{14,12},{16,18},{18,... | collective-permute-start | bytes 1966088 | tf_op jit(solution)/shard_map/ppermute | solution.py:302
  119.4 7.4 %copy-start.9 = (bf16[160,2048]{1,0:T(8,128)(2,1)}, bf16[160,2048]{1,0:T(8,128)(2,1)S(1)}, u32[]{:S(2)}) copy-start(bf16[160,2048]{1,0:T(8,128)(2,1)S(1)} %collective-permute-done.26.cot_ref.refs_3_) | copy-start | bytes 1966084
  123.8 3.1 %copy-start.11 = (bf16[160,2048]{1,0:T(8,128)(2,1)}, bf16[160,2048]{1,0:T(8,128)(2,1)S(1)}, u32[]{:S(2)}) copy-start(bf16[160,2048]{1,0:T(8,128)(2,1)S(1)} %collective-permute-done.25.tok_ref.refs_3_) | copy-start | bytes 1966084
  128.9 3.4 %copy-start.23 = (f32[8,128]{1,0:T(8,128)}, f32[8,128]{1,0:T(8,128)S(1)}, u32[]{:S(2)}) copy-start(f32[8,128]{1,0:T(8,128)S(1)} %get-tuple-element.73.refs_3_) | copy-start | bytes 12292
  128.9 6.9 %collective-permute-start.33 = (bf16[160,2048]{1,0:T(8,128)(2,1)S(1)}, bf16[160,2048]{1,0:T(8,128)(2,1)S(1)}, u32[]{:S(2)}, u32[]{:S(2)}) collective-permute-start(bf16[160,2048]{1,0:T(8,128)(2,1)S(1)} %get-tuple-element.84), channel_id=1, source_target_pairs={{0,2},{2,0},{4,6},{6,4},{8,10},{10,8},{12,14},{14,12},{16,18},{18,... | collective-permute-start | bytes 1966088 | tf_op jit(solution)/shard_map/ppermute | solution.py:302
  138.8 25.0 %collective-permute-start.34 = (bf16[80,1024]{1,0:T(8,128)(2,1)}, bf16[80,1024]{1,0:T(8,128)(2,1)S(1)}, u32[]{:S(2)}, u32[]{:S(2)}) collective-permute-start(bf16[80,1024]{1,0:T(8,128)(2,1)} %get-tuple-element.86), channel_id=1, source_target_pairs={{0,1},{1,0},{2,3},{3,2},{4,5},{5,4},{6,7},{7,6},{8,9},{9,8},{10,11... | collective-permute-start | bytes 491528 | tf_op jit(solution)/shard_map/ppermute | solution.py:317
  140.3 23.5 %collective-permute-start.35 = (bf16[80,1024]{1,0:T(8,128)(2,1)}, bf16[80,1024]{1,0:T(8,128)(2,1)S(1)}, u32[]{:S(2)}, u32[]{:S(2)}) collective-permute-start(bf16[80,1024]{1,0:T(8,128)(2,1)} %get-tuple-element.87), channel_id=1, source_target_pairs={{0,4},{1,5},{2,6},{3,7},{4,0},{5,1},{6,2},{7,3},{8,12},{9,13},{10,... | collective-permute-start | bytes 491528 | tf_op jit(solution)/shard_map/ppermute | solution.py:317
  141.8 22.0 %collective-permute-start.36 = (bf16[80,1024]{1,0:T(8,128)(2,1)}, bf16[80,1024]{1,0:T(8,128)(2,1)S(1)}, u32[]{:S(2)}, u32[]{:S(2)}) collective-permute-start(bf16[80,1024]{1,0:T(8,128)(2,1)} %get-tuple-element.88), channel_id=1, source_target_pairs={{0,5},{1,4},{2,7},{3,6},{4,1},{5,0},{6,3},{7,2},{8,13},{9,12},{10,... | collective-permute-start | bytes 491528 | tf_op jit(solution)/shard_map/ppermute | solution.py:317
  142.3 1.6 copy-start.3
  143.9 1.6 copy-start.6
  145.5 18.3 %copy-start.17 = (bf16[80,1024]{1,0:T(8,128)(2,1)S(1)}, bf16[80,1024]{1,0:T(8,128)(2,1)}, u32[]{:S(2)}) copy-start(bf16[80,1024]{1,0:T(8,128)(2,1)} %get-tuple-element.85.refs_0_) | copy-start | bytes 491524
  159.6 10.6 %all-to-all-start = ((f32[16,1,128]{2,1,0:T(1,128)}), f32[16,1,128]{2,1,0:T(1,128)S(1)}, u32[]{:S(2)}, u32[]{:S(2)}) async-start(f32[16,1,128]{2,1,0:T(1,128)} %shard_map.124), calls=%async_computation | async-start | bytes 16384 | tf_op jit(solution)/shard_map/all_to_all | solution.py:455
  163.9 47.4 %collective-permute-start.37 = (bf16[80,1024]{1,0:T(8,128)(2,1)S(1)}, bf16[80,1024]{1,0:T(8,128)(2,1)S(1)}, u32[]{:S(2)}, u32[]{:S(2)}) collective-permute-start(bf16[80,1024]{1,0:T(8,128)(2,1)S(1)} %shard_map.129), channel_id=1, source_target_pairs={{0,16},{2,18},{4,20},{6,22},{8,24},{10,26},{12,28},{14,30},{16,0},... | collective-permute-start | bytes 491528 | tf_op jit(solution)/shard_map/ppermute | solution.py:306
  170.3 5.1 %copy-start.36 = (f32[4,128]{1,0:T(4,128)}, f32[4,128]{1,0:T(4,128)S(1)}, u32[]{:S(2)}) copy-start(f32[4,128]{1,0:T(4,128)S(1)} %reduce_sum.18.refs_0_) | copy-start | bytes 6148
  170.3 18.5 %collective-permute-start.27 = (f32[4,128]{1,0:T(4,128)S(1)}, f32[4,128]{1,0:T(4,128)S(1)}, u32[]{:S(2)}, u32[]{:S(2)}) collective-permute-start(f32[4,128]{1,0:T(4,128)S(1)} %reduce_sum.18.refs_0_), channel_id=1, source_target_pairs={{0,1},{1,0},{2,3},{3,2},{4,5},{5,4},{6,7},{7,6},{8,9},{9,8},{10,11... | collective-permute-start | bytes 6152 | tf_op jit(solution)/shard_map/ppermute | solution.py:309
  175.4 19.7 %collective-permute-start.29 = (bf16[240,1024]{1,0:T(8,128)(2,1)}, bf16[240,1024]{1,0:T(8,128)(2,1)S(1)}, u32[]{:S(2)}, u32[]{:S(2)}) collective-permute-start(bf16[240,1024]{1,0:T(8,128)(2,1)} %get-tuple-element.78), channel_id=1, source_target_pairs={{0,1},{1,0},{2,3},{3,2},{4,5},{5,4},{6,7},{7,6},{8,9},{9,8},{10,11... | collective-permute-start | bytes 1474568 | tf_op jit(solution)/shard_map/ppermute | solution.py:317
  175.9 19.2 %collective-permute-start.30 = (bf16[240,1024]{1,0:T(8,128)(2,1)}, bf16[240,1024]{1,0:T(8,128)(2,1)S(1)}, u32[]{:S(2)}, u32[]{:S(2)}) collective-permute-start(bf16[240,1024]{1,0:T(8,128)(2,1)} %get-tuple-element.79), channel_id=1, source_target_pairs={{0,4},{1,5},{2,6},{3,7},{4,0},{5,1},{6,2},{7,3},{8,12},{9,13},{10,... | collective-permute-start | bytes 1474568 | tf_op jit(solution)/shard_map/ppermute | solution.py:317
  176.2 23.9 %collective-permute-start.31 = (bf16[240,1024]{1,0:T(8,128)(2,1)}, bf16[240,1024]{1,0:T(8,128)(2,1)S(1)}, u32[]{:S(2)}, u32[]{:S(2)}) collective-permute-start(bf16[240,1024]{1,0:T(8,128)(2,1)} %get-tuple-element.80), channel_id=1, source_target_pairs={{0,5},{1,4},{2,7},{3,6},{4,1},{5,0},{6,3},{7,2},{8,13},{9,12},{10,... | collective-permute-start | bytes 1474568 | tf_op jit(solution)/shard_map/ppermute | solution.py:317
  178.9 21.2 %copy-start.13 = (bf16[240,1024]{1,0:T(8,128)(2,1)S(1)}, bf16[240,1024]{1,0:T(8,128)(2,1)}, u32[]{:S(2)}) copy-start(bf16[240,1024]{1,0:T(8,128)(2,1)} %get-tuple-element.77.refs_0_) | copy-start | bytes 1474564
  191.6 19.1 %all-to-all-start.1 = ((f32[16,4,128]{2,1,0:T(4,128)}), f32[16,4,128]{2,1,0:T(4,128)S(1)}, u32[]{:S(2)}, u32[]{:S(2)}) async-start(f32[16,4,128]{2,1,0:T(4,128)} %get-tuple-element.91), calls=%async_computation.1 | async-start | bytes 65536 | tf_op jit(solution)/shard_map/all_to_all | solution.py:471
  200.4 10.9 %collective-permute-start.32 = (bf16[80,1024]{1,0:T(8,128)(2,1)S(1)}, bf16[80,1024]{1,0:T(8,128)(2,1)S(1)}, u32[]{:S(2)}, u32[]{:S(2)}) collective-permute-start(bf16[80,1024]{1,0:T(8,128)(2,1)S(1)} %get-tuple-element.82), channel_id=1, source_target_pairs={{0,24},{2,26},{4,28},{6,30},{8,0},{10,2},{12,4},{14,6},{16,8},{18,... | collective-permute-start | bytes 491528 | tf_op jit(solution)/shard_map/ppermute | solution.py:306
  200.8 10.5 %collective-permute-start.38 = (bf16[80,1024]{1,0:T(8,128)(2,1)S(1)}, bf16[80,1024]{1,0:T(8,128)(2,1)S(1)}, u32[]{:S(2)}, u32[]{:S(2)}) collective-permute-start(bf16[80,1024]{1,0:T(8,128)(2,1)S(1)} %get-tuple-element.89), channel_id=1, source_target_pairs={{0,8},{2,10},{4,12},{6,14},{8,16},{10,18},{12,20},{14,22},{16,24},... | collective-permute-start | bytes 491528 | tf_op jit(solution)/shard_map/ppermute | solution.py:306
  202.4 8.8 %copy-start.16 = (bf16[4,80,128]{2,1,0:T(8,128)(2,1)S(1)}, bf16[4,80,128]{2,1,0:T(8,128)(2,1)}, u32[]{:S(2)}) copy-start(bf16[4,80,128]{2,1,0:T(8,128)(2,1)} %get-tuple-element.56.place_ref) | copy-start | bytes 245764
  202.4 8.8 %copy-start.20 = (bf16[2048,4]{0,1:T(4,128)(2,1)S(1)}, bf16[2048,4]{0,1:T(4,128)(2,1)}, u32[]{:S(2)}) copy-start(bf16[2048,4]{0,1:T(4,128)(2,1)} %param.9) | copy-start | bytes 49156
  202.4 8.8 %copy-start.21 = (s32[3]{0:T(128)S(1)}, s32[3]{0:T(128)}, u32[]{:S(2)}) copy-start(s32[3]{0:T(128)} %pad_add_fusion.at_ref) | copy-start | bytes 40
  202.5 8.9 %copy-start.26 = (f32[4,128]{1,0:T(4,128)S(1)}, f32[4,128]{1,0:T(4,128)}, u32[]{:S(2)}) copy-start(f32[4,128]{1,0:T(4,128)} %get-tuple-element.74.change_ref) | copy-start | bytes 6148
  (17 other events, 12.7 us)
